TPU v7x, 128 devices: a whole 4x4x4 slice. The times are simulated.
128 devices in a mesh: ep: 64 (over z, y, x), tp: 2 (over core).
Axes of the slice: x: 4, y: 4, z: 4, core: 2. Of those that a mesh axis runs over, the one named last changes fastest.
Arguments:
- tokens: bfloat16 [1024, 2048], P('ep'), may hold values from -6 to 6
- attn_gain: float32 [2048], replicated, may hold values from 0.1 to 1.9
- w_query1: bfloat16 [2048, 512], P(None, 'tp'), may hold values from -0.125 to 0.125
- w_query2: bfloat16 [2048, 512], P(None, 'tp'), may hold values from -0.125 to 0.125
- w_key1: bfloat16 [2048, 128], P(None, 'tp'), may hold values from -0.125 to 0.125
- w_key2: bfloat16 [2048, 128], P(None, 'tp'), may hold values from -0.125 to 0.125
- w_value: bfloat16 [2048, 256], P(None, 'tp'), may hold values from -0.125 to 0.125
- query_gain: float32 [64], replicated, may hold values from 1.1 to 1.6
- key_gain: float32 [64], replicated, may hold values from 1.1 to 1.6
- head_lambda: float32 [8], P('tp'), may hold values from 0.3 to 0.8
- sub_gain: float32 [128], replicated, may hold values from 0.1 to 1.9
- w_output: bfloat16 [1024, 2048], P('tp'), may hold values from -0.1875 to 0.1875
- cache_key: bfloat16 [1024, 2, 1024, 128], P('ep', 'tp'), may hold values from -300 to 300
- cache_value: bfloat16 [1024, 2, 1024, 128], P('ep', 'tp'), may hold values from -6 to 6
- lengths: int32 [1024], P('ep'), may hold values from 1 to 1024, 524288 in all
- mix_gain: float32 [2048], replicated, may hold values from 0.1 to 1.9
- expert_gate: bfloat16 [64, 2048, 1536], P('ep', None, 'tp'), may hold values from -0.375 to 0.375
- expert_up: bfloat16 [64, 2048, 1536], P('ep', None, 'tp'), may hold values from -0.375 to 0.375
- expert_down: bfloat16 [64, 1536, 2048], P('ep', 'tp'), may hold values from -0.0546875 to 0.0546875
- routes: int32 [1024, 4], P('ep'), may hold values from 0 to 63, all different within a row; in each aligned block of 16 rows (0 to 15, 16 to 31, ...) at most 2 rows name the same one
- route_weight: bfloat16 [1024, 4], P('ep'), may hold values from 0.049804688 to 0.59765625
- dense_mix: bfloat16 [2048], replicated, may hold values from -0.125 to 0.125
- dense_gate: bfloat16 [2048, 4096], P(None, ('ep', 'tp')), may hold values from -0.375 to 0.375
- dense_up: bfloat16 [2048, 4096], P(None, ('ep', 'tp')), may hold values from -0.375 to 0.375
- dense_down: bfloat16 [4096, 2048], P(('ep', 'tp')), may hold values from -0.03125 to 0.03125
Outputs:
- layer_out: bfloat16 [1024, 2048], P('ep', 'tp')
Inputs may be any that keep to these rules, and one draw needn't show every extreme that they name: `lengths`: each sequence has at least one cached position in use; some sequence uses all 1024. `routes`: each row names 4 different experts; among the rows of one index of ep no expert is named by more than 2 rows, and in some such block one expert is named by exactly 2.
All inputs are finite; a program needn't handle non-finite values. No bound on the sum of `lengths` on one device may be relied on, other than what follows from the above.
Results may differ from a plain program's by a relative error of at most 0.018.
The roundings to bfloat16 on the way count: a program that leaves them out, or rounds other values in their place, can miss the bound.
Values may be sent and summed in bfloat16 or wider, within the bound.
No kernel may reach another device: no remote copies, remote signals or barrier semaphores. Data moves between devices by JAX's collectives and lax.ppermute only.
A program may use at most 128 MiB of HBM per device.

v0:
```python
import functools

import jax
import jax.numpy as jnp
from jax import lax
from jax.experimental import pallas as pl
from jax.experimental.pallas import tpu as pltpu
from jax.sharding import Mesh
from jax.sharding import PartitionSpec as P


HEAD = 64
VHEAD = 128
EP = ("ep_0", "ep_1", "ep_2")
EP_TP = ("ep_0", "ep_1", "ep_2", "tp")
SLOTS = 6
CAP = 2
DENSE_ROWS = 4
LANES = 128
SEQ_STEP = 4
LIMIT = 40 << 20

epsilon = 1e-05
clamp_limit = 7.0
sigmoid_slope = 1.702
lambda_start = 0.2
neg_large = -1e30

bf16 = jnp.bfloat16
f32 = jnp.float32
NT = (((1,), (1,)), ((), ()))
TN = (((0,), (0,)), ((), ()))


def mm(a, b, dims=(((1,), (0,)), ((), ()))):
    return lax.dot_general(a, b, dims, preferred_element_type=f32)


def clamped_unit(gate_pre, up_pre):
    gate_pre = jnp.minimum(gate_pre, clamp_limit)
    up_pre = jnp.clip(up_pre, -clamp_limit, clamp_limit)
    return gate_pre * jax.nn.sigmoid(sigmoid_slope * gate_pre) * (up_pre + 1.0)


def rms(values):
    return lax.rsqrt(jnp.mean(values * values, axis=-1, keepdims=True) + epsilon)


def routing_maps(routes_t, weight_t, seqs, peers):
    wide = peers * SLOTS
    diag = lax.broadcasted_iota(jnp.int32, (seqs, seqs), 0) == lax.broadcasted_iota(
        jnp.int32, (seqs, seqs), 1
    )
    lane = lax.broadcasted_iota(jnp.int32, (seqs, wide), 1)
    peer, slot = lane % peers, lane // peers
    token = lax.broadcasted_iota(jnp.int32, (seqs, wide), 0)
    hit = jnp.zeros((seqs, wide), f32)
    weight = jnp.zeros((seqs, wide), f32)
    for k in range(routes_t.shape[0]):
        expert = jnp.sum(
            jnp.where(diag, routes_t[k : k + 1, :].astype(f32), 0.0), axis=1, keepdims=True
        ).astype(jnp.int32)
        share = jnp.sum(
            jnp.where(diag, weight_t[k : k + 1, :].astype(f32), 0.0), axis=1, keepdims=True
        )
        same = peer == expert
        hit = jnp.where(same, 1.0, hit)
        weight = jnp.where(same, share, weight)
    before = (
        lax.broadcasted_iota(jnp.int32, (seqs, seqs), 1)
        < lax.broadcasted_iota(jnp.int32, (seqs, seqs), 0)
    ).astype(bf16)
    rank = mm(before, hit.astype(bf16))
    chosen = (hit > 0.0) & (rank == slot.astype(f32)) & (slot < CAP)
    group = 2 * ((peer // 16) % 2) + (peer // 4) % 2
    dense = (token == group * DENSE_ROWS + slot - CAP) & (slot >= CAP)
    return (
        jnp.where(chosen | dense, 1.0, 0.0).astype(bf16),
        jnp.where(chosen, weight, 0.0).astype(bf16),
        jnp.where(dense, 1.0, 0.0).astype(bf16),
    )


def attention_kernel(*refs, peers):
    sources, refs = refs[:17], refs[17:]
    part, send_map, home_map = refs[:3]
    query_s, key_s, value_s, heads_s, *local = refs[3:-1]
    sems = refs[-1]
    (
        lengths, lam, tokens, attn_gain, w_query1, w_query2, w_key1, w_key2, w_value, query_gain, key_gain,
        routes_t, weight_t, sub_gain, w_output, cache_key, cache_value,
    ) = local
    seqs = tokens.shape[0]
    heads = w_query1.shape[1] // HEAD
    cached = cache_key.shape[2]
    rounds = seqs // SEQ_STEP
    copies = [
        pltpu.make_async_copy(sources[i], local[i], sems.at[i]) for i in range(len(local) - 2)
    ]
    chunks = []
    for b in range(rounds):
        of = pl.ds(b * SEQ_STEP, SEQ_STEP)
        for j in (0, 1):
            at = len(copies) + len(chunks)
            source, to = sources[15 + j].at[of], local[15 + j].at[of]
            chunks.append(pltpu.make_async_copy(source, to, sems.at[at]))
    for one in copies[:-1] + chunks + copies[-1:]:
        one.start()

    for one in copies[:-1]:
        one.wait()
    rows = tokens[...].astype(f32)
    normed = (rows * rms(rows) * attn_gain[...]).astype(bf16)
    nothing = jnp.zeros((seqs, HEAD), f32)
    for m, weight in enumerate((w_query1, w_query2)):
        query = mm(normed, weight[...])
        for h in range(heads):
            one = query[:, h * HEAD : (h + 1) * HEAD]
            one = (one * rms(one) * query_gain[...]).astype(bf16).astype(f32) * HEAD**-0.5
            pair = (one, nothing) if m == 0 else (nothing, one)
            at = (m * heads + h) * seqs
            query_s[at : at + seqs, :] = jnp.concatenate(pair, axis=1)
    new_keys = []
    for weight in (w_key1, w_key2):
        one = mm(normed, weight[...], NT)
        new_keys.append((one * rms(one) * key_gain[...]).astype(bf16).astype(f32))
    key_s[...] = jnp.concatenate(new_keys, axis=1)
    value_s[...] = mm(normed, w_value[...]).astype(bf16).astype(f32)
    send, routed, dense = routing_maps(routes_t[...], weight_t[...], seqs, peers)
    send_map[...] = send
    home_map[0:seqs, :] = routed
    home_map[seqs : 2 * seqs, :] = dense

    row = lax.broadcasted_iota(jnp.int32, (2 * heads, 1), 0)
    signed = jnp.ones((2 * heads, 1), f32)
    for h in range(heads):
        signed = jnp.where(row == heads + h, -lam[h], signed)
    lane = lax.broadcasted_iota(jnp.int32, (2 * heads, cached), 1)
    for b in range(rounds):
        chunks[2 * b].wait()
        chunks[2 * b + 1].wait()
        for s in range(b * SEQ_STEP, (b + 1) * SEQ_STEP):
            query = query_s[pl.ds(s, 2 * heads, stride=seqs), :]
            fresh = jnp.sum(query * key_s[s : s + 1, :], axis=1, keepdims=True)
            scores = mm(query.astype(bf16), cache_key[s, 0], NT)
            scores = jnp.where(lane < lengths[s], scores, neg_large)
            top = jnp.maximum(jnp.max(scores, axis=1, keepdims=True), fresh)
            expo = jnp.exp(scores - top)
            fresh_expo = jnp.exp(fresh - top)
            scale = signed / (jnp.sum(expo, axis=1, keepdims=True) + fresh_expo)
            probs = expo * scale
            probs = (probs + pltpu.roll(probs, heads, 0)).astype(bf16)
            fresh_probs = fresh_expo * scale
            fresh_probs = fresh_probs[0:heads] + fresh_probs[heads:]
            heads_out = mm(probs, cache_value[s, 0])[0:heads]
            heads_out = heads_out + fresh_probs.astype(bf16).astype(f32) * value_s[s : s + 1, :]
            heads_s[pl.ds(s, heads, stride=seqs), :] = heads_out

    subs = []
    for h in range(heads):
        one = heads_s[h * seqs : (h + 1) * seqs, :]
        subs.append((one * rms(one) * sub_gain[...] * (1.0 - lambda_start)).astype(bf16))
    copies[-1].wait()
    part[...] = mm(jnp.concatenate(subs, axis=1), w_output[...]).astype(bf16)


def attention(
    tokens, attn_gain, w_query1, w_query2, w_key1, w_key2, w_value, query_gain, key_gain,
    head_lambda, sub_gain, w_output, cache_key, cache_value, lengths, routes, route_weight,
    peers,
):
    seqs, width = tokens.shape
    heads = w_query1.shape[1] // HEAD
    cached = cache_key.shape[2]
    local = [
        lengths, head_lambda, tokens, attn_gain.reshape(1, -1), w_query1, w_query2, w_key1.T, w_key2.T, w_value,
        query_gain.reshape(1, -1), key_gain.reshape(1, -1), routes.T, route_weight.T,
        sub_gain.reshape(1, -1), w_output, cache_key, cache_value,
    ]
    flops = 2 * seqs * width * (2 * heads * HEAD + 2 * HEAD + VHEAD + heads * VHEAD)
    flops += 6 * seqs * 8 * cached * VHEAD
    wide = peers * SLOTS
    count = len(local) - 2 + 2 * (seqs // SEQ_STEP)
    return pl.pallas_call(
        functools.partial(attention_kernel, peers=peers),
        in_specs=[pl.BlockSpec(memory_space=pltpu.HBM)] * len(local),
        out_specs=[pl.BlockSpec(memory_space=pltpu.VMEM)] * 3,
        out_shape=[
            pltpu.VMEM((seqs, width), bf16),
            pltpu.VMEM((seqs, wide), bf16),
            pltpu.VMEM((2 * seqs, wide), bf16),
        ],
        scratch_shapes=[
            pltpu.VMEM((2 * heads * seqs, 2 * HEAD), f32),
            pltpu.VMEM((seqs, 2 * HEAD), f32),
            pltpu.VMEM((seqs, VHEAD), f32),
            pltpu.VMEM((heads * seqs, VHEAD), f32),
        ]
        + [pltpu.SMEM(one.shape, one.dtype) for one in local[:2]]
        + [pltpu.VMEM(one.shape, one.dtype) for one in local[2:]]
        + [pltpu.SemaphoreType.DMA((count,))],
        compiler_params=pltpu.CompilerParams(vmem_limit_bytes=LIMIT),
        cost_estimate=pl.CostEstimate(
            flops=flops, bytes_accessed=13 << 20, transcendentals=seqs * 8 * cached
        ),
        name="attention",
    )(*[pltpu.with_memory_space_constraint(one, pltpu.HBM) for one in local])


def spread(wide_s, rows, first):
    slots, peers, parts = wide_s.shape[0] // 64 // 8, 64, rows.shape[1] // LANES
    for r in range(rows.shape[0] // peers):
        for c in range(parts):
            wide_s[pl.ds((first + r) * parts + c, peers, stride=slots * parts), :] = rows[
                r * peers : (r + 1) * peers, c * LANES : (c + 1) * LANES
            ]


def gather(wide_s, r, c, parts, peers):
    slots = wide_s.shape[0] // peers // parts
    return wide_s[pl.ds(r * parts + c, peers, stride=slots * parts), :].astype(bf16)


def mix_kernel(core, tokens, mine, other, mix_gain, dense_mix, send_map, send, kept, row_gate, wide_s):
    half = kept.shape[1]
    attn_out = mine[...].astype(f32) + other[...].astype(f32)
    residual = (tokens[...].astype(f32) + attn_out).astype(bf16)
    rows = residual.astype(f32)
    mixed = (rows * rms(rows) * mix_gain[...]).astype(bf16).astype(f32)
    first = core[0] == 0
    kept[...] = jnp.where(first, rows[:, :half], rows[:, half:])
    gate = jnp.zeros((rows.shape[0], LANES), f32)
    for c in range(rows.shape[1] // LANES):
        gate = gate + mixed[:, c * LANES : (c + 1) * LANES] * dense_mix[c : c + 1, :].astype(f32)
    gate = jnp.sum(gate, axis=1, keepdims=True)
    row_gate[...] = jnp.broadcast_to(jax.nn.sigmoid(gate), row_gate.shape)
    columns = jnp.where(first, mixed[:, :half], mixed[:, half:]).astype(bf16)
    spread(wide_s, mm(send_map[...], columns, TN), 0)
    send[...] = wide_s[...].astype(bf16)


def call(kernel, args, outs, scratch, flops, transcendentals=0, far=0):
    near = len(args) - far
    spaces = [pltpu.SMEM if one.ndim == 1 else pltpu.VMEM for one in args[:near]]
    spaces += [pltpu.HBM] * far
    args = list(args[:near]) + [
        pltpu.with_memory_space_constraint(one, pltpu.HBM) for one in args[near:]
    ]
    out_shape = [jax.ShapeDtypeStruct(*one) for one in outs]
    moved = sum(one.size * one.dtype.itemsize for one in args + out_shape)
    return pl.pallas_call(
        kernel,
        in_specs=[pl.BlockSpec(memory_space=space) for space in spaces],
        out_specs=[pl.BlockSpec(memory_space=pltpu.VMEM)] * len(outs),
        out_shape=out_shape,
        scratch_shapes=[pltpu.VMEM(*one) for one in scratch]
        + [pltpu.SemaphoreType.DMA((far,))] * (far > 0),
        compiler_params=pltpu.CompilerParams(vmem_limit_bytes=LIMIT // 2),
        cost_estimate=pl.CostEstimate(
            flops=flops, bytes_accessed=moved, transcendentals=transcendentals
        ),
    )(*args)


def compact(wide_s, rows_e, rows_d):
    parts, peers = rows_d.shape[1] // LANES, rows_e.shape[0] // CAP
    for r in range(SLOTS):
        for c in range(parts):
            to, at = (rows_e, r) if r < CAP else (rows_d, r - CAP)
            to[at * peers : (at + 1) * peers, c * LANES : (c + 1) * LANES] = gather(
                wide_s, r, c, parts, peers
            )


def first_kernel(
    core, mine, gate_far, up_far, rows_d, gate_part, up_part, wide_s, rows_e, gate, up, sems
):
    half = rows_d.shape[1]
    own = pl.ds(pl.multiple_of(core[0] * half, half), half)
    fetch_gate = pltpu.make_async_copy(gate_far.at[0, own], gate, sems.at[0])
    fetch_up = pltpu.make_async_copy(up_far.at[0, own], up, sems.at[1])
    fetch_gate.start()
    fetch_up.start()
    wide_s[...] = mine[...].astype(f32)
    compact(wide_s, rows_e, rows_d)
    fetch_gate.wait()
    gate_part[...] = mm(rows_e[...], gate[...])
    fetch_up.wait()
    up_part[...] = mm(rows_e[...], up[...])


def second_kernel(
    core, other, gate_part, up_part, gate_far, up_far, down_far, rows_d, out_mine, out_other,
    wide_s, rows_e, total, gate, up, down, sems,
):
    half = rows_d.shape[1]
    at = pl.multiple_of(core[0] * half, half)
    back = pl.multiple_of((1 - core[0]) * half, half)
    fetch_gate = pltpu.make_async_copy(gate_far.at[0, pl.ds(back, half)], gate, sems.at[0])
    fetch_up = pltpu.make_async_copy(up_far.at[0, pl.ds(back, half)], up, sems.at[1])
    fetch_down = pltpu.make_async_copy(down_far.at[0], down, sems.at[2])
    fetch_gate.start()
    fetch_up.start()
    fetch_down.start()
    wide_s[...] = other[...].astype(f32)
    compact(wide_s, rows_e, rows_d)
    fetch_gate.wait()
    gate_pre = gate_part[...] + mm(rows_e[...], gate[...])
    fetch_up.wait()
    up_pre = up_part[...] + mm(rows_e[...], up[...])
    hidden = clamped_unit(gate_pre, up_pre).astype(bf16)
    fetch_down.wait()
    total[...] = mm(hidden, down[...])
    out_mine[...] = total[:, pl.ds(at, half)].astype(bf16)
    out_other[...] = total[:, pl.ds(back, half)].astype(bf16)


def dense_kernel(core, mine, other, *refs):
    packs, out, gate_s, up_s, down_s = refs[:-4], refs[-4], refs[-3], refs[-2], refs[-1]
    half = mine.shape[1]
    units = packs[0].shape[0] // 3
    at = pl.multiple_of(core[0] * half, half)
    back = pl.multiple_of((1 - core[0]) * half, half)
    for i, pack in enumerate(packs):
        to = slice(i * units, (i + 1) * units)
        gate_s[to, :] = pack[0:units, :]
        up_s[to, :] = pack[units : 2 * units, :]
        down_s[to, :] = pack[2 * units : 3 * units, pl.ds(at, half)]
    rows, far = mine[...], other[...]
    gate = mm(rows, gate_s[:, pl.ds(at, half)], NT) + mm(far, gate_s[:, pl.ds(back, half)], NT)
    up = mm(rows, up_s[:, pl.ds(at, half)], NT) + mm(far, up_s[:, pl.ds(back, half)], NT)
    out[...] = mm(clamped_unit(gate, up).astype(bf16), down_s[...])


def join_kernel(dense, mine, other, out, wide_s):
    total = (mine[...].astype(f32) + other[...].astype(f32)).astype(bf16).astype(f32)
    spread(wide_s, total, 0)
    spread(wide_s, dense[...], CAP)
    out[...] = wide_s[...].astype(bf16)


def home_kernel(home_map, returned, kept, row_gate, out, wide_s, rows_s):
    seqs, half = kept.shape
    parts = half // LANES
    peers = rows_s.shape[0] // SLOTS
    wide_s[...] = returned[...].astype(f32)
    for r in range(SLOTS):
        for c in range(parts):
            rows_s[r * peers : (r + 1) * peers, c * LANES : (c + 1) * LANES] = gather(
                wide_s, r, c, parts, peers
            )
    sums = mm(home_map[...], rows_s[...])
    out[...] = (kept[...] + sums[:seqs] + row_gate[:, 0:1] * sums[seqs:]).astype(bf16)


def swap(array):
    return lax.ppermute(array, "tp", [(0, 1), (1, 0)])


def from_square(array):
    got = []
    for flip0, flip1 in ((1, 0), (0, 1), (1, 1)):
        pairs = [(4 * a + b, 4 * (a ^ flip0) + (b ^ flip1)) for a in range(4) for b in range(4)]
        got.append(lax.ppermute(array, ("ep_0", "ep_1"), pairs))
    return got


def shards(
    tokens, attn_gain, w_query1, w_query2, w_key1, w_key2, w_value, query_gain, key_gain,
    head_lambda, sub_gain, w_output, cache_key, cache_value, lengths, mix_gain, expert_gate,
    expert_up, expert_down, routes, route_weight, dense_mix, dense_gate, dense_up, dense_down,
):
    peers = lax.axis_size(EP)
    seqs, width = tokens.shape
    half, slots, wide = width // 2, CAP * peers, SLOTS * peers
    hidden = expert_gate.shape[2]
    core = lax.axis_index("tp").astype(jnp.int32).reshape(1)
    pack = jnp.concatenate([dense_gate.T, dense_up.T, dense_down], axis=0)
    packs = [pack] + from_square(pack)
    part, send_map, home_map = attention(
        tokens, attn_gain, w_query1, w_query2, w_key1, w_key2, w_value, query_gain,
        key_gain, head_lambda, sub_gain, w_output, cache_key, cache_value, lengths,
        routes, route_weight, peers,
    )
    block = (wide * half // LANES, LANES)
    send, kept, row_gate = call(
        mix_kernel,
        (
            core, tokens, part, swap(part), mix_gain.reshape(1, -1),
            dense_mix.reshape(-1, LANES), send_map,
        ),
        [(block, bf16), ((seqs, half), f32), ((seqs, LANES), f32)],
        [(block, f32)],
        2 * wide * seqs * half,
    )

    def exchange(blocks):
        blocks = blocks.reshape(peers, -1, LANES)
        return lax.all_to_all(blocks, EP, 0, 0, tiled=True).reshape(block)

    mine = exchange(send)
    other = swap(mine)
    rows_mine, gate_part, up_part = call(
        first_kernel,
        (core, mine, expert_gate, expert_up),
        [((DENSE_ROWS * peers, half), bf16)] + [((slots, hidden), f32)] * 2,
        [(block, f32), ((slots, half), bf16)] + [((half, hidden), bf16)] * 2,
        4 * slots * half * hidden,
        far=2,
    )
    rows_other, own, sent = call(
        second_kernel,
        (core, other, gate_part, up_part, expert_gate, expert_up, expert_down),
        [((DENSE_ROWS * peers, half), bf16)] + [((slots, half), bf16)] * 2,
        [(block, f32), ((slots, half), bf16), ((slots, width), f32)]
        + [((half, hidden), bf16)] * 2
        + [((hidden, width), bf16)],
        8 * slots * half * hidden,
        slots * hidden,
        far=3,
    )
    came = swap(sent)
    packs = packs + [swap(one) for one in packs]
    units = pack.shape[0] // 3 * len(packs)
    (dense,) = call(
        dense_kernel,
        (core, rows_mine, rows_other, *packs),
        [((DENSE_ROWS * peers, half), f32)],
        [((units, width), bf16), ((units, width), bf16), ((units, half), bf16)],
        10 * DENSE_ROWS * peers * half * units,
        DENSE_ROWS * peers * units,
    )
    (joined,) = call(join_kernel, (dense, own, came), [(block, bf16)], [(block, f32)], 0)
    returned = exchange(joined)
    (out,) = call(
        home_kernel,
        (home_map, returned, kept, row_gate),
        [((seqs, half), bf16)],
        [(block, f32), ((wide, half), bf16)],
        4 * seqs * wide * half,
    )
    return out


def solution(mesh):
    torus = Mesh(mesh.devices.reshape(4, 4, 4, mesh.shape["tp"]), EP_TP)
    in_specs = (
        P(EP, None), P(), P(None, "tp"), P(None, "tp"), P(None, "tp"), P(None, "tp"),
        P(None, "tp"), P(), P(), P("tp"), P(), P("tp", None), P(EP, "tp", None, None),
        P(EP, "tp", None, None), P(EP), P(), P(EP, None, "tp"), P(EP, None, "tp"),
        P(EP, "tp", None), P(EP, None), P(EP, None), P(), P(None, EP_TP), P(None, EP_TP),
        P(EP_TP, None),
    )
    return jax.shard_map(
        shards, mesh=torus, in_specs=in_specs, out_specs=P(EP, "tp"), check_vma=False
    )
```

profile of v0, /device:TPU:0, one launch (start us, length us, event | category | flops | bytes accessed | tf_op | source)
XLA Modules:
  0.0 92.1 jit_solution(12632825486415739141)
XLA Ops:
  0.0 10.1 %attention.1 = (bf16[16,2048]{1,0:T(8,128)(2,1)S(1)}, bf16[16,384]{1,0:T(8,128)(2,1)S(1)}, bf16[32,384]{1,0:T(8,128)(2,1)S(1)}) custom-call(s32[16]{0:T(128)} %refs_0_.1, f32[4]{0:T(128)} %refs_1_.1, bf16[16,2048]{1,0:T(8,128)(2,1)} %tokens.1, f32[1,2048]{1,0:T(1,128)} %bitcast.28, bf16[2048,256]{1,0:T(8,128)(2,1)} %refs_4_.1, bf16[2048,256]{1,0:T(8,128)(2,1)} %refs_5_.1, ...), custom_call_target="tpu_custom_call" | custom-call | flops 184549376 | bytes 13631488 | tf_op jit(solution)/shard_map/attention/pallas_call | solution.py:184
  10.1 0.1 collective-permute-start
  10.2 1.2 %collective-permute-done.other = bf16[16,2048]{1,0:T(8,128)(2,1)S(1)} collective-permute-done((bf16[16,2048]{1,0:T(8,128)(2,1)S(1)}, bf16[16,2048]{1,0:T(8,128)(2,1)S(1)}, u32[]{:S(2)}, u32[]{:S(2)}) %collective-permute-start) | collective-permute-done | bytes 65568 | tf_op jit(solution)/shard_map/ppermute | solution.py:357
  11.5 0.8 shard_map.235
  12.3 27.8 %all_to_all.10 = bf16[64,48,128]{2,1,0:T(8,128)(2,1)S(1)} all-to-all(bf16[64,48,128]{2,1,0:T(8,128)(2,1)S(1)} %bitcast.21), channel_id=1, replica_groups=mesh['ep_0'=4,'ep_1'=4,'ep_2'=4,'tp'=2] {'ep_0','ep_1','ep_2'}, dimensions={0} | all-to-all | bytes 1572864 | tf_op jit(solution)/shard_map/all_to_all | solution.py:399
  40.2 0.5 collective-permute-start.2
  40.7 0.2 collective-permute-start.3
  40.9 2.8 %collective-permute-start.4 = (bf16[96,2048]{1,0:T(8,128)(2,1)S(1)}, bf16[96,2048]{1,0:T(8,128)(2,1)S(1)}, u32[]{:S(2)}, u32[]{:S(2)}) collective-permute-start(bf16[96,2048]{1,0:T(8,128)(2,1)S(1)} %pad_maximum_fusion.refs_0_), channel_id=1, source_target_pairs={{0,40},{8,32},{16,56},{24,48},{32,8},{40,0},{48,24},{56,16},{64,10... | collective-permute-start | bytes 1179656 | tf_op jit(solution)/shard_map/ppermute | solution.py:364
  43.7 0.0 collective-permute-start.5
  43.7 8.0 %collective-permute-done.2.refs_1_ = bf16[96,2048]{1,0:T(8,128)(2,1)S(1)} collective-permute-done((bf16[96,2048]{1,0:T(8,128)(2,1)S(1)}, bf16[96,2048]{1,0:T(8,128)(2,1)S(1)}, u32[]{:S(2)}, u32[]{:S(2)}) %collective-permute-start.2) | collective-permute-done | bytes 393248 | tf_op jit(solution)/shard_map/ppermute | solution.py:364
  51.8 0.9 %collective-permute-done.3.refs_2_ = bf16[96,2048]{1,0:T(8,128)(2,1)S(1)} collective-permute-done((bf16[96,2048]{1,0:T(8,128)(2,1)S(1)}, bf16[96,2048]{1,0:T(8,128)(2,1)S(1)}, u32[]{:S(2)}, u32[]{:S(2)}) %collective-permute-start.3) | collective-permute-done | bytes 393248 | tf_op jit(solution)/shard_map/ppermute | solution.py:364
  52.7 0.0 collective-permute-start.7
  52.7 8.7 %collective-permute-done.4.refs_3_ = bf16[96,2048]{1,0:T(8,128)(2,1)S(1)} collective-permute-done((bf16[96,2048]{1,0:T(8,128)(2,1)S(1)}, bf16[96,2048]{1,0:T(8,128)(2,1)S(1)}, u32[]{:S(2)}, u32[]{:S(2)}) %collective-permute-start.4) | collective-permute-done | bytes 393248 | tf_op jit(solution)/shard_map/ppermute | solution.py:364
  61.4 0.0 collective-permute-start.8
  61.4 2.3 %shard_map.236 = (bf16[256,1024]{1,0:T(8,128)(2,1)S(1)}, f32[128,768]{1,0:T(8,128)S(1)}, f32[128,768]{1,0:T(8,128)S(1)}) custom-call(s32[1]{0:T(128)} %bitcast.8.core, bf16[3072,128]{1,0:T(8,128)(2,1)S(1)} %bitcast.18, bf16[1,2048,768]{2,1,0:T(8,128)(2,1)} %gate_far.3, bf16[1,2048,768]{2,1,0:T(8,128)(2,1)} %up_far.3), custom_call_target="tpu_custom_call" | custom-call | flops 402653184 | bytes 8388612 | tf_op jit(solution)/shard_map/pallas_call | solution.py:251
  63.7 0.0 collective-permute-done.1.other
  63.7 3.5 %shard_map.237 = (bf16[256,1024]{1,0:T(8,128)(2,1)S(1)}, bf16[128,1024]{1,0:T(8,128)(2,1)S(1)}, bf16[128,1024]{1,0:T(8,128)(2,1)S(1)}) custom-call(s32[1]{0:T(128)} %bitcast.8.core, bf16[3072,128]{1,0:T(8,128)(2,1)S(1)} %collective-permute-done.1.other, f32[128,768]{1,0:T(8,128)S(1)} %get-tuple-element.22.gate_part, ...), custom_call_target="tpu_custom_call" | custom-call | flops 805306368 | bytes 12058628 | tf_op jit(solution)/shard_map/pallas_call | solution.py:251
  67.2 0.6 collective-permute-start.9
  67.8 0.0 collective-permute-done.6.refs_5_
  67.9 1.1 %shard_map.238.dense = f32[256,1024]{1,0:T(8,128)S(1)} custom-call(s32[1]{0:T(128)} %bitcast.8.core, bf16[256,1024]{1,0:T(8,128)(2,1)S(1)} %get-tuple-element.21.mine, bf16[256,1024]{1,0:T(8,128)(2,1)S(1)} %get-tuple-element.24.other, bf16[96,2048]{1,0:T(8,128)(2,1)S(1)} %pad_maximum_fusion.refs_0_, bf16[96,2048]{1,0:T(8,128)(2,1)S(1)} %collective-permute-done.2.refs_1_, ...), custom_call_target="tpu_custom_call" | custom-call | flops 671088640 | bytes 5242884 | tf_op jit(solution)/shard_map/pallas_call | solution.py:251
  69.0 0.0 collective-permute-done.9.other
  69.0 0.6 shard_map.239
  69.6 21.1 %all_to_all.11 = bf16[64,48,128]{2,1,0:T(8,128)(2,1)S(1)} all-to-all(bf16[64,48,128]{2,1,0:T(8,128)(2,1)S(1)} %bitcast.20), channel_id=1, replica_groups=mesh['ep_0'=4,'ep_1'=4,'ep_2'=4,'tp'=2] {'ep_0','ep_1','ep_2'}, dimensions={0} | all-to-all | bytes 1572864 | tf_op jit(solution)/shard_map/all_to_all | solution.py:399
  90.7 1.5 %shard_map.240 = bf16[16,1024]{1,0:T(8,128)(2,1)} custom-call(bf16[32,384]{1,0:T(8,128)(2,1)S(1)} %get-tuple-element.17.home_map, bf16[3072,128]{1,0:T(8,128)(2,1)S(1)} %bitcast.19, f32[16,1024]{1,0:T(8,128)S(1)} %get-tuple-element.27.kept, f32[16,128]{1,0:T(8,128)S(1)} %get-tuple-element.28.row_gate), custom_call_target="tpu_custom_call" | custom-call | flops 25165824 | bytes 917504 | tf_op jit(solution)/shard_map/pallas_call | solution.py:251
  (18 shorter events, 0.1 us)
Async XLA Ops:
  0.0 11.5 %copy-start = (bf16[16,2048]{1,0:T(8,128)(2,1)S(1)}, bf16[16,2048]{1,0:T(8,128)(2,1)}, u32[]{:S(2)}) copy-start(bf16[16,2048]{1,0:T(8,128)(2,1)} %tokens.1) | copy-start | bytes 196612
  0.0 11.5 %copy-start.1 = (f32[2048]{0:T(1024)S(1)}, f32[2048]{0:T(1024)}, u32[]{:S(2)}) copy-start(f32[2048]{0:T(1024)} %param.40) | copy-start | bytes 24580
  0.0 11.5 %copy-start.2 = (bf16[2048]{0:T(1024)(128)(2,1)S(1)}, bf16[2048]{0:T(1024)(128)(2,1)}, u32[]{:S(2)}) copy-start(bf16[2048]{0:T(1024)(128)(2,1)} %param.46) | copy-start | bytes 12292
  0.0 40.1 %copy-start.3 = (bf16[32,2048]{1,0:T(8,128)(2,1)S(1)}, bf16[32,2048]{1,0:T(8,128)(2,1)}, u32[]{:S(2)}) copy-start(bf16[32,2048]{1,0:T(8,128)(2,1)} %param.49) | copy-start | bytes 393220
  0.0 40.1 %copy-start.4 = (bf16[2048,32]{0,1:T(8,128)(2,1)S(1)}, bf16[2048,32]{0,1:T(8,128)(2,1)}, u32[]{:S(2)}) copy-start(bf16[2048,32]{0,1:T(8,128)(2,1)} %param.48) | copy-start | bytes 393220
  0.0 40.1 %copy-start.5 = (bf16[2048,32]{0,1:T(8,128)(2,1)S(1)}, bf16[2048,32]{0,1:T(8,128)(2,1)}, u32[]{:S(2)}) copy-start(bf16[2048,32]{0,1:T(8,128)(2,1)} %param.47) | copy-start | bytes 393220
  10.1 1.3 %collective-permute-start = (bf16[16,2048]{1,0:T(8,128)(2,1)S(1)}, bf16[16,2048]{1,0:T(8,128)(2,1)S(1)}, u32[]{:S(2)}, u32[]{:S(2)}) collective-permute-start(bf16[16,2048]{1,0:T(8,128)(2,1)S(1)} %get-tuple-element.18.mine), channel_id=1, source_target_pairs={{0,1},{1,0},{2,3},{3,2},{4,5},{5,4},{6,7},{7,6},{8,9},{9,8},{10,11... | collective-permute-start | bytes 196616 | tf_op jit(solution)/shard_map/ppermute | solution.py:357
  40.1 23.6 %collective-permute-start.1 = (bf16[3072,128]{1,0:T(8,128)(2,1)S(1)}, bf16[3072,128]{1,0:T(8,128)(2,1)S(1)}, u32[]{:S(2)}, u32[]{:S(2)}) collective-permute-start(bf16[3072,128]{1,0:T(8,128)(2,1)S(1)} %bitcast.17), channel_id=1, source_target_pairs={{0,1},{1,0},{2,3},{3,2},{4,5},{5,4},{6,7},{7,6},{8,9},{9,8},{10,11... | collective-permute-start | bytes 2359304 | tf_op jit(solution)/shard_map/ppermute | solution.py:357
  40.2 11.6 %collective-permute-start.2 = (bf16[96,2048]{1,0:T(8,128)(2,1)S(1)}, bf16[96,2048]{1,0:T(8,128)(2,1)S(1)}, u32[]{:S(2)}, u32[]{:S(2)}) collective-permute-start(bf16[96,2048]{1,0:T(8,128)(2,1)S(1)} %pad_maximum_fusion.refs_0_), channel_id=1, source_target_pairs={{0,32},{8,40},{16,48},{24,56},{32,0},{40,8},{48,16},{56,24},{64,96... | collective-permute-start | bytes 1179656 | tf_op jit(solution)/shard_map/ppermute | solution.py:364
  40.7 12.0 %collective-permute-start.3 = (bf16[96,2048]{1,0:T(8,128)(2,1)S(1)}, bf16[96,2048]{1,0:T(8,128)(2,1)S(1)}, u32[]{:S(2)}, u32[]{:S(2)}) collective-permute-start(bf16[96,2048]{1,0:T(8,128)(2,1)S(1)} %pad_maximum_fusion.refs_0_), channel_id=1, source_target_pairs={{0,8},{8,0},{16,24},{24,16},{32,40},{40,32},{48,56},{56,48},{64,72... | collective-permute-start | bytes 1179656 | tf_op jit(solution)/shard_map/ppermute | solution.py:364
  40.9 20.4 %collective-permute-start.4 = (bf16[96,2048]{1,0:T(8,128)(2,1)S(1)}, bf16[96,2048]{1,0:T(8,128)(2,1)S(1)}, u32[]{:S(2)}, u32[]{:S(2)}) collective-permute-start(bf16[96,2048]{1,0:T(8,128)(2,1)S(1)} %pad_maximum_fusion.refs_0_), channel_id=1, source_target_pairs={{0,40},{8,32},{16,56},{24,48},{32,8},{40,0},{48,24},{56,16},{64,10... | collective-permute-start | bytes 1179656 | tf_op jit(solution)/shard_map/ppermute | solution.py:364
  43.7 24.1 %collective-permute-start.5 = (bf16[96,2048]{1,0:T(8,128)(2,1)S(1)}, bf16[96,2048]{1,0:T(8,128)(2,1)S(1)}, u32[]{:S(2)}, u32[]{:S(2)}) collective-permute-start(bf16[96,2048]{1,0:T(8,128)(2,1)S(1)} %pad_maximum_fusion.refs_0_), channel_id=1, source_target_pairs={{0,1},{1,0},{2,3},{3,2},{4,5},{5,4},{6,7},{7,6},{8,9},{9,8},{10,11... | collective-permute-start | bytes 1179656 | tf_op jit(solution)/shard_map/ppermute | solution.py:357
  51.7 16.1 %collective-permute-start.6 = (bf16[96,2048]{1,0:T(8,128)(2,1)S(1)}, bf16[96,2048]{1,0:T(8,128)(2,1)S(1)}, u32[]{:S(2)}, u32[]{:S(2)}) collective-permute-start(bf16[96,2048]{1,0:T(8,128)(2,1)S(1)} %collective-permute-done.2.refs_1_), channel_id=1, source_target_pairs={{0,1},{1,0},{2,3},{3,2},{4,5},{5,4},{6,7},{7,6},{8,9},{9,8},{10,11... | collective-permute-start | bytes 1179656 | tf_op jit(solution)/shard_map/ppermute | solution.py:357
  52.7 15.2 %collective-permute-start.7 = (bf16[96,2048]{1,0:T(8,128)(2,1)S(1)}, bf16[96,2048]{1,0:T(8,128)(2,1)S(1)}, u32[]{:S(2)}, u32[]{:S(2)}) collective-permute-start(bf16[96,2048]{1,0:T(8,128)(2,1)S(1)} %collective-permute-done.3.refs_2_), channel_id=1, source_target_pairs={{0,1},{1,0},{2,3},{3,2},{4,5},{5,4},{6,7},{7,6},{8,9},{9,8},{10,11... | collective-permute-start | bytes 1179656 | tf_op jit(solution)/shard_map/ppermute | solution.py:357
  61.4 6.5 %collective-permute-start.8 = (bf16[96,2048]{1,0:T(8,128)(2,1)S(1)}, bf16[96,2048]{1,0:T(8,128)(2,1)S(1)}, u32[]{:S(2)}, u32[]{:S(2)}) collective-permute-start(bf16[96,2048]{1,0:T(8,128)(2,1)S(1)} %collective-permute-done.4.refs_3_), channel_id=1, source_target_pairs={{0,1},{1,0},{2,3},{3,2},{4,5},{5,4},{6,7},{7,6},{8,9},{9,8},{10,11... | collective-permute-start | bytes 1179656 | tf_op jit(solution)/shard_map/ppermute | solution.py:357
  67.2 1.8 %collective-permute-start.9 = (bf16[128,1024]{1,0:T(8,128)(2,1)S(1)}, bf16[128,1024]{1,0:T(8,128)(2,1)S(1)}, u32[]{:S(2)}, u32[]{:S(2)}) collective-permute-start(bf16[128,1024]{1,0:T(8,128)(2,1)S(1)} %get-tuple-element.26), channel_id=1, source_target_pairs={{0,1},{1,0},{2,3},{3,2},{4,5},{5,4},{6,7},{7,6},{8,9},{9,8},{10,11... | collective-permute-start | bytes 786440 | tf_op jit(solution)/shard_map/ppermute | solution.py:357
where the time goes:
time: 92.3 us; the launch traced here: 92.1 us
  blocking collectives  48.9 us (53%)
  Pallas kernels  19.9 us (22%)
  waiting for transfers between devices  18.9 us (20%)
  starting transfers between devices  4.26 us (5%)
    all_to_all x2, blocking collectives, exchange(): return lax.all_to_all(blocks, EP, 0, 0, tiled=True).reshape(block)  48.9 us
    ppermute x3, waiting for transfers between devices, from_square(): got.append(lax.ppermute(array, ('ep_0', 'ep_1'), pairs))  17.6 us
    pallas_call x1, Pallas kernels, attention(): pl.pallas_call(functools.partial(attention_kernel, peers=peers), in_specs...  10.1 us
    pallas_call x6, Pallas kernels, call(): pl.pallas_call(kernel, in_specs=[pl.BlockSpec(memory_space=space) for spa...  9.81 us
    ppermute x3, starting transfers between devices, from_square(): got.append(lax.ppermute(array, ('ep_0', 'ep_1'), pairs))  3.57 us
  transfers between devices with their start and end apart: 10, of which 4 were waited for; matrix products, arithmetic and copies ran while one was open for 0% of the time, Pallas kernels for 8%

commit v1 on v0

--- a/solution.py
+++ b/solution.py
@@ -17,7 +17,7 @@
 CAP = 2
 DENSE_ROWS = 4
 LANES = 128
-SEQ_STEP = 4
+SEQ_STEP = 8
 LIMIT = 40 << 20
 
 epsilon = 1e-05
@@ -137,23 +137,34 @@
         signed = jnp.where(row == heads + h, -lam[h], signed)
     lane = lax.broadcasted_iota(jnp.int32, (2 * heads, cached), 1)
     for b in range(rounds):
+        span = range(b * SEQ_STEP, (b + 1) * SEQ_STEP)
         chunks[2 * b].wait()
+        queries = [query_s[pl.ds(s, 2 * heads, stride=seqs), :] for s in span]
+        fresh = [
+            jnp.sum(query * key_s[s : s + 1, :], axis=1, keepdims=True)
+            for s, query in zip(span, queries)
+        ]
+        scores = [
+            jnp.where(lane < lengths[s], mm(query.astype(bf16), cache_key[s, 0], NT), neg_large)
+            for s, query in zip(span, queries)
+        ]
+        top = [
+            jnp.maximum(jnp.max(one, axis=1, keepdims=True), new)
+            for one, new in zip(scores, fresh)
+        ]
+        expo = [jnp.exp(one - most) for one, most in zip(scores, top)]
+        fresh_expo = [jnp.exp(one - most) for one, most in zip(fresh, top)]
+        scale = [
+            signed / (jnp.sum(one, axis=1, keepdims=True) + new)
+            for one, new in zip(expo, fresh_expo)
+        ]
+        probs = [one * by for one, by in zip(expo, scale)]
+        probs = [(one + pltpu.roll(one, heads, 0)).astype(bf16) for one in probs]
         chunks[2 * b + 1].wait()
-        for s in range(b * SEQ_STEP, (b + 1) * SEQ_STEP):
-            query = query_s[pl.ds(s, 2 * heads, stride=seqs), :]
-            fresh = jnp.sum(query * key_s[s : s + 1, :], axis=1, keepdims=True)
-            scores = mm(query.astype(bf16), cache_key[s, 0], NT)
-            scores = jnp.where(lane < lengths[s], scores, neg_large)
-            top = jnp.maximum(jnp.max(scores, axis=1, keepdims=True), fresh)
-            expo = jnp.exp(scores - top)
-            fresh_expo = jnp.exp(fresh - top)
-            scale = signed / (jnp.sum(expo, axis=1, keepdims=True) + fresh_expo)
-            probs = expo * scale
-            probs = (probs + pltpu.roll(probs, heads, 0)).astype(bf16)
-            fresh_probs = fresh_expo * scale
-            fresh_probs = fresh_probs[0:heads] + fresh_probs[heads:]
-            heads_out = mm(probs, cache_value[s, 0])[0:heads]
-            heads_out = heads_out + fresh_probs.astype(bf16).astype(f32) * value_s[s : s + 1, :]
+        for s, one, new, by in zip(span, probs, fresh_expo, scale):
+            new = new * by
+            new = (new[0:heads] + new[heads:]).astype(bf16).astype(f32)
+            heads_out = mm(one, cache_value[s, 0])[0:heads] + new * value_s[s : s + 1, :]
             heads_s[pl.ds(s, heads, stride=seqs), :] = heads_out
 
     subs = []

time: 92.3 us -> 88.1 us (0.954)
  Pallas kernels: 19.9 us -> 15.8 us
    pallas_call x1, Pallas kernels: 10.1 us -> 5.95 us  [attention(): pl.pallas_call(functools.partial(attention_kernel, peers=peers), in_specs...]
where the time goes in v1:
time: 88.1 us; the launch traced here: 88 us
  blocking collectives  48.9 us (56%)
  waiting for transfers between devices  18.9 us (21%)
  Pallas kernels  15.8 us (18%)
  starting transfers between devices  4.26 us (5%)
    all_to_all x2, blocking collectives, exchange(): return lax.all_to_all(blocks, EP, 0, 0, tiled=True).reshape(block)  48.9 us
    ppermute x3, waiting for transfers between devices, from_square(): got.append(lax.ppermute(array, ('ep_0', 'ep_1'), pairs))  17.6 us
    pallas_call x6, Pallas kernels, call(): pl.pallas_call(kernel, in_specs=[pl.BlockSpec(memory_space=space) for spa...  9.8 us
    pallas_call x1, Pallas kernels, attention(): pl.pallas_call(functools.partial(attention_kernel, peers=peers), in_specs...  5.95 us
    ppermute x3, starting transfers between devices, from_square(): got.append(lax.ppermute(array, ('ep_0', 'ep_1'), pairs))  3.57 us
  transfers between devices with their start and end apart: 10, of which 4 were waited for; matrix products, arithmetic and copies ran while one was open for 0% of the time, Pallas kernels for 8%

profile of v1, /device:TPU:0, one launch (start us, length us, event | category | flops | bytes accessed | tf_op | source)
XLA Modules:
  0.0 88.0 jit_solution(2381449624708952810)
XLA Ops:
  0.0 5.9 %attention.1 = (bf16[16,2048]{1,0:T(8,128)(2,1)S(1)}, bf16[16,384]{1,0:T(8,128)(2,1)S(1)}, bf16[32,384]{1,0:T(8,128)(2,1)S(1)}) custom-call(s32[16]{0:T(128)} %refs_0_.1, f32[4]{0:T(128)} %refs_1_.1, bf16[16,2048]{1,0:T(8,128)(2,1)} %tokens.1, f32[1,2048]{1,0:T(1,128)} %bitcast.28, bf16[2048,256]{1,0:T(8,128)(2,1)} %refs_4_.1, bf16[2048,256]{1,0:T(8,128)(2,1)} %refs_5_.1, ...), custom_call_target="tpu_custom_call" | custom-call | flops 184549376 | bytes 13631488 | tf_op jit(solution)/shard_map/attention/pallas_call | solution.py:195
  6.0 0.1 collective-permute-start
  6.1 1.2 %collective-permute-done.other = bf16[16,2048]{1,0:T(8,128)(2,1)S(1)} collective-permute-done((bf16[16,2048]{1,0:T(8,128)(2,1)S(1)}, bf16[16,2048]{1,0:T(8,128)(2,1)S(1)}, u32[]{:S(2)}, u32[]{:S(2)}) %collective-permute-start) | collective-permute-done | bytes 65568 | tf_op jit(solution)/shard_map/ppermute | solution.py:368
  7.3 0.8 shard_map.235
  8.1 27.8 %all_to_all.10 = bf16[64,48,128]{2,1,0:T(8,128)(2,1)S(1)} all-to-all(bf16[64,48,128]{2,1,0:T(8,128)(2,1)S(1)} %bitcast.21), channel_id=1, replica_groups=mesh['ep_0'=4,'ep_1'=4,'ep_2'=4,'tp'=2] {'ep_0','ep_1','ep_2'}, dimensions={0} | all-to-all | bytes 1572864 | tf_op jit(solution)/shard_map/all_to_all | solution.py:410
  35.9 0.0 collective-permute-start.1
  36.0 0.5 collective-permute-start.2
  36.5 0.2 collective-permute-start.3
  36.8 2.8 %collective-permute-start.4 = (bf16[96,2048]{1,0:T(8,128)(2,1)S(1)}, bf16[96,2048]{1,0:T(8,128)(2,1)S(1)}, u32[]{:S(2)}, u32[]{:S(2)}) collective-permute-start(bf16[96,2048]{1,0:T(8,128)(2,1)S(1)} %pad_maximum_fusion.refs_0_), channel_id=1, source_target_pairs={{0,40},{8,32},{16,56},{24,48},{32,8},{40,0},{48,24},{56,16},{64,10... | collective-permute-start | bytes 1179656 | tf_op jit(solution)/shard_map/ppermute | solution.py:375
  39.6 8.0 %collective-permute-done.2.refs_1_ = bf16[96,2048]{1,0:T(8,128)(2,1)S(1)} collective-permute-done((bf16[96,2048]{1,0:T(8,128)(2,1)S(1)}, bf16[96,2048]{1,0:T(8,128)(2,1)S(1)}, u32[]{:S(2)}, u32[]{:S(2)}) %collective-permute-start.2) | collective-permute-done | bytes 393248 | tf_op jit(solution)/shard_map/ppermute | solution.py:375
  47.6 0.9 %collective-permute-done.3.refs_2_ = bf16[96,2048]{1,0:T(8,128)(2,1)S(1)} collective-permute-done((bf16[96,2048]{1,0:T(8,128)(2,1)S(1)}, bf16[96,2048]{1,0:T(8,128)(2,1)S(1)}, u32[]{:S(2)}, u32[]{:S(2)}) %collective-permute-start.3) | collective-permute-done | bytes 393248 | tf_op jit(solution)/shard_map/ppermute | solution.py:375
  48.5 0.0 collective-permute-start.7
  48.5 8.7 %collective-permute-done.4.refs_3_ = bf16[96,2048]{1,0:T(8,128)(2,1)S(1)} collective-permute-done((bf16[96,2048]{1,0:T(8,128)(2,1)S(1)}, bf16[96,2048]{1,0:T(8,128)(2,1)S(1)}, u32[]{:S(2)}, u32[]{:S(2)}) %collective-permute-start.4) | collective-permute-done | bytes 393248 | tf_op jit(solution)/shard_map/ppermute | solution.py:375
  57.2 0.0 collective-permute-start.8
  57.2 2.3 %shard_map.236 = (bf16[256,1024]{1,0:T(8,128)(2,1)S(1)}, f32[128,768]{1,0:T(8,128)S(1)}, f32[128,768]{1,0:T(8,128)S(1)}) custom-call(s32[1]{0:T(128)} %bitcast.8.core, bf16[3072,128]{1,0:T(8,128)(2,1)S(1)} %bitcast.18, bf16[1,2048,768]{2,1,0:T(8,128)(2,1)} %gate_far.3, bf16[1,2048,768]{2,1,0:T(8,128)(2,1)} %up_far.3), custom_call_target="tpu_custom_call" | custom-call | flops 402653184 | bytes 8388612 | tf_op jit(solution)/shard_map/pallas_call | solution.py:262
  59.5 0.0 collective-permute-done.1.other
  59.6 3.5 %shard_map.237 = (bf16[256,1024]{1,0:T(8,128)(2,1)S(1)}, bf16[128,1024]{1,0:T(8,128)(2,1)S(1)}, bf16[128,1024]{1,0:T(8,128)(2,1)S(1)}) custom-call(s32[1]{0:T(128)} %bitcast.8.core, bf16[3072,128]{1,0:T(8,128)(2,1)S(1)} %collective-permute-done.1.other, f32[128,768]{1,0:T(8,128)S(1)} %get-tuple-element.22.gate_part, ...), custom_call_target="tpu_custom_call" | custom-call | flops 805306368 | bytes 12058628 | tf_op jit(solution)/shard_map/pallas_call | solution.py:262
  63.1 0.6 collective-permute-start.9
  63.7 0.0 collective-permute-done.8.refs_7_
  63.7 1.1 %shard_map.238.dense = f32[256,1024]{1,0:T(8,128)S(1)} custom-call(s32[1]{0:T(128)} %bitcast.8.core, bf16[256,1024]{1,0:T(8,128)(2,1)S(1)} %get-tuple-element.21.mine, bf16[256,1024]{1,0:T(8,128)(2,1)S(1)} %get-tuple-element.24.other, bf16[96,2048]{1,0:T(8,128)(2,1)S(1)} %pad_maximum_fusion.refs_0_, bf16[96,2048]{1,0:T(8,128)(2,1)S(1)} %collective-permute-done.2.refs_1_, ...), custom_call_target="tpu_custom_call" | custom-call | flops 671088640 | bytes 5242884 | tf_op jit(solution)/shard_map/pallas_call | solution.py:262
  64.8 0.0 collective-permute-done.9.other
  64.8 0.6 shard_map.239
  65.4 21.1 %all_to_all.11 = bf16[64,48,128]{2,1,0:T(8,128)(2,1)S(1)} all-to-all(bf16[64,48,128]{2,1,0:T(8,128)(2,1)S(1)} %bitcast.20), channel_id=1, replica_groups=mesh['ep_0'=4,'ep_1'=4,'ep_2'=4,'tp'=2] {'ep_0','ep_1','ep_2'}, dimensions={0} | all-to-all | bytes 1572864 | tf_op jit(solution)/shard_map/all_to_all | solution.py:410
  86.5 1.5 %shard_map.240 = bf16[16,1024]{1,0:T(8,128)(2,1)} custom-call(bf16[32,384]{1,0:T(8,128)(2,1)S(1)} %get-tuple-element.17.home_map, bf16[3072,128]{1,0:T(8,128)(2,1)S(1)} %bitcast.19, f32[16,1024]{1,0:T(8,128)S(1)} %get-tuple-element.27.kept, f32[16,128]{1,0:T(8,128)S(1)} %get-tuple-element.28.row_gate), custom_call_target="tpu_custom_call" | custom-call | flops 25165824 | bytes 917504 | tf_op jit(solution)/shard_map/pallas_call | solution.py:262
  (18 shorter events, 0.1 us)
Async XLA Ops:
  0.0 7.3 %copy-start = (bf16[16,2048]{1,0:T(8,128)(2,1)S(1)}, bf16[16,2048]{1,0:T(8,128)(2,1)}, u32[]{:S(2)}) copy-start(bf16[16,2048]{1,0:T(8,128)(2,1)} %tokens.1) | copy-start | bytes 196612
  0.0 7.3 %copy-start.1 = (f32[2048]{0:T(1024)S(1)}, f32[2048]{0:T(1024)}, u32[]{:S(2)}) copy-start(f32[2048]{0:T(1024)} %param.40) | copy-start | bytes 24580
  0.0 7.3 %copy-start.2 = (bf16[2048]{0:T(1024)(128)(2,1)S(1)}, bf16[2048]{0:T(1024)(128)(2,1)}, u32[]{:S(2)}) copy-start(bf16[2048]{0:T(1024)(128)(2,1)} %param.46) | copy-start | bytes 12292
  0.0 35.9 %copy-start.3 = (bf16[32,2048]{1,0:T(8,128)(2,1)S(1)}, bf16[32,2048]{1,0:T(8,128)(2,1)}, u32[]{:S(2)}) copy-start(bf16[32,2048]{1,0:T(8,128)(2,1)} %param.49) | copy-start | bytes 393220
  0.0 35.9 %copy-start.4 = (bf16[2048,32]{0,1:T(8,128)(2,1)S(1)}, bf16[2048,32]{0,1:T(8,128)(2,1)}, u32[]{:S(2)}) copy-start(bf16[2048,32]{0,1:T(8,128)(2,1)} %param.48) | copy-start | bytes 393220
  0.0 35.9 %copy-start.5 = (bf16[2048,32]{0,1:T(8,128)(2,1)S(1)}, bf16[2048,32]{0,1:T(8,128)(2,1)}, u32[]{:S(2)}) copy-start(bf16[2048,32]{0,1:T(8,128)(2,1)} %param.47) | copy-start | bytes 393220
  6.0 1.3 %collective-permute-start = (bf16[16,2048]{1,0:T(8,128)(2,1)S(1)}, bf16[16,2048]{1,0:T(8,128)(2,1)S(1)}, u32[]{:S(2)}, u32[]{:S(2)}) collective-permute-start(bf16[16,2048]{1,0:T(8,128)(2,1)S(1)} %get-tuple-element.18.mine), channel_id=1, source_target_pairs={{0,1},{1,0},{2,3},{3,2},{4,5},{5,4},{6,7},{7,6},{8,9},{9,8},{10,11... | collective-permute-start | bytes 196616 | tf_op jit(solution)/shard_map/ppermute | solution.py:368
  35.9 23.6 %collective-permute-start.1 = (bf16[3072,128]{1,0:T(8,128)(2,1)S(1)}, bf16[3072,128]{1,0:T(8,128)(2,1)S(1)}, u32[]{:S(2)}, u32[]{:S(2)}) collective-permute-start(bf16[3072,128]{1,0:T(8,128)(2,1)S(1)} %bitcast.17), channel_id=1, source_target_pairs={{0,1},{1,0},{2,3},{3,2},{4,5},{5,4},{6,7},{7,6},{8,9},{9,8},{10,11... | collective-permute-start | bytes 2359304 | tf_op jit(solution)/shard_map/ppermute | solution.py:368
  36.0 11.6 %collective-permute-start.2 = (bf16[96,2048]{1,0:T(8,128)(2,1)S(1)}, bf16[96,2048]{1,0:T(8,128)(2,1)S(1)}, u32[]{:S(2)}, u32[]{:S(2)}) collective-permute-start(bf16[96,2048]{1,0:T(8,128)(2,1)S(1)} %pad_maximum_fusion.refs_0_), channel_id=1, source_target_pairs={{0,32},{8,40},{16,48},{24,56},{32,0},{40,8},{48,16},{56,24},{64,96... | collective-permute-start | bytes 1179656 | tf_op jit(solution)/shard_map/ppermute | solution.py:375
  36.5 12.0 %collective-permute-start.3 = (bf16[96,2048]{1,0:T(8,128)(2,1)S(1)}, bf16[96,2048]{1,0:T(8,128)(2,1)S(1)}, u32[]{:S(2)}, u32[]{:S(2)}) collective-permute-start(bf16[96,2048]{1,0:T(8,128)(2,1)S(1)} %pad_maximum_fusion.refs_0_), channel_id=1, source_target_pairs={{0,8},{8,0},{16,24},{24,16},{32,40},{40,32},{48,56},{56,48},{64,72... | collective-permute-start | bytes 1179656 | tf_op jit(solution)/shard_map/ppermute | solution.py:375
  36.8 20.4 %collective-permute-start.4 = (bf16[96,2048]{1,0:T(8,128)(2,1)S(1)}, bf16[96,2048]{1,0:T(8,128)(2,1)S(1)}, u32[]{:S(2)}, u32[]{:S(2)}) collective-permute-start(bf16[96,2048]{1,0:T(8,128)(2,1)S(1)} %pad_maximum_fusion.refs_0_), channel_id=1, source_target_pairs={{0,40},{8,32},{16,56},{24,48},{32,8},{40,0},{48,24},{56,16},{64,10... | collective-permute-start | bytes 1179656 | tf_op jit(solution)/shard_map/ppermute | solution.py:375
  39.6 24.1 %collective-permute-start.5 = (bf16[96,2048]{1,0:T(8,128)(2,1)S(1)}, bf16[96,2048]{1,0:T(8,128)(2,1)S(1)}, u32[]{:S(2)}, u32[]{:S(2)}) collective-permute-start(bf16[96,2048]{1,0:T(8,128)(2,1)S(1)} %pad_maximum_fusion.refs_0_), channel_id=1, source_target_pairs={{0,1},{1,0},{2,3},{3,2},{4,5},{5,4},{6,7},{7,6},{8,9},{9,8},{10,11... | collective-permute-start | bytes 1179656 | tf_op jit(solution)/shard_map/ppermute | solution.py:368
  47.6 16.1 %collective-permute-start.6 = (bf16[96,2048]{1,0:T(8,128)(2,1)S(1)}, bf16[96,2048]{1,0:T(8,128)(2,1)S(1)}, u32[]{:S(2)}, u32[]{:S(2)}) collective-permute-start(bf16[96,2048]{1,0:T(8,128)(2,1)S(1)} %collective-permute-done.2.refs_1_), channel_id=1, source_target_pairs={{0,1},{1,0},{2,3},{3,2},{4,5},{5,4},{6,7},{7,6},{8,9},{9,8},{10,11... | collective-permute-start | bytes 1179656 | tf_op jit(solution)/shard_map/ppermute | solution.py:368
  48.5 15.2 %collective-permute-start.7 = (bf16[96,2048]{1,0:T(8,128)(2,1)S(1)}, bf16[96,2048]{1,0:T(8,128)(2,1)S(1)}, u32[]{:S(2)}, u32[]{:S(2)}) collective-permute-start(bf16[96,2048]{1,0:T(8,128)(2,1)S(1)} %collective-permute-done.3.refs_2_), channel_id=1, source_target_pairs={{0,1},{1,0},{2,3},{3,2},{4,5},{5,4},{6,7},{7,6},{8,9},{9,8},{10,11... | collective-permute-start | bytes 1179656 | tf_op jit(solution)/shard_map/ppermute | solution.py:368
  57.2 6.5 %collective-permute-start.8 = (bf16[96,2048]{1,0:T(8,128)(2,1)S(1)}, bf16[96,2048]{1,0:T(8,128)(2,1)S(1)}, u32[]{:S(2)}, u32[]{:S(2)}) collective-permute-start(bf16[96,2048]{1,0:T(8,128)(2,1)S(1)} %collective-permute-done.4.refs_3_), channel_id=1, source_target_pairs={{0,1},{1,0},{2,3},{3,2},{4,5},{5,4},{6,7},{7,6},{8,9},{9,8},{10,11... | collective-permute-start | bytes 1179656 | tf_op jit(solution)/shard_map/ppermute | solution.py:368
  63.1 1.8 %collective-permute-start.9 = (bf16[128,1024]{1,0:T(8,128)(2,1)S(1)}, bf16[128,1024]{1,0:T(8,128)(2,1)S(1)}, u32[]{:S(2)}, u32[]{:S(2)}) collective-permute-start(bf16[128,1024]{1,0:T(8,128)(2,1)S(1)} %get-tuple-element.26), channel_id=1, source_target_pairs={{0,1},{1,0},{2,3},{3,2},{4,5},{5,4},{6,7},{7,6},{8,9},{9,8},{10,11... | collective-permute-start | bytes 786440 | tf_op jit(solution)/shard_map/ppermute | solution.py:368

commit v2 on v1

--- a/solution.py
+++ b/solution.py
@@ -368,12 +368,15 @@
     return lax.ppermute(array, "tp", [(0, 1), (1, 0)])
 
 
-def from_square(array):
-    got = []
-    for flip0, flip1 in ((1, 0), (0, 1), (1, 1)):
-        pairs = [(4 * a + b, 4 * (a ^ flip0) + (b ^ flip1)) for a in range(4) for b in range(4)]
-        got.append(lax.ppermute(array, ("ep_0", "ep_1"), pairs))
-    return got
+def across(array, turn):
+    pairs = []
+    for a in range(4):
+        for b in range(4):
+            for t in range(2):
+                flip = (t + turn) % 2
+                to = 4 * (a ^ (1 - flip)) + (b ^ flip)
+                pairs.append((2 * (4 * a + b) + t, 2 * to + t))
+    return lax.ppermute(array, ("ep_0", "ep_1", "tp"), pairs)
 
 
 def shards(
@@ -387,17 +390,20 @@
     hidden = expert_gate.shape[2]
     core = lax.axis_index("tp").astype(jnp.int32).reshape(1)
     pack = jnp.concatenate([dense_gate.T, dense_up.T, dense_down], axis=0)
-    packs = [pack] + from_square(pack)
+    pack0 = across(pack, 0)
     part, send_map, home_map = attention(
         tokens, attn_gain, w_query1, w_query2, w_key1, w_key2, w_value, query_gain,
         key_gain, head_lambda, sub_gain, w_output, cache_key, cache_value, lengths,
         routes, route_weight, peers,
     )
     block = (wide * half // LANES, LANES)
+    far = swap(part)
+    pack1 = across(pack, 1)
+    pack2 = across(pack0, 1)
     send, kept, row_gate = call(
         mix_kernel,
         (
-            core, tokens, part, swap(part), mix_gain.reshape(1, -1),
+            core, tokens, part, far, mix_gain.reshape(1, -1),
             dense_mix.reshape(-1, LANES), send_map,
         ),
         [(block, bf16), ((seqs, half), f32), ((seqs, LANES), f32)],
@@ -431,6 +437,7 @@
         far=3,
     )
     came = swap(sent)
+    packs = [pack, pack0, pack1, pack2]
     packs = packs + [swap(one) for one in packs]
     units = pack.shape[0] // 3 * len(packs)
     (dense,) = call(

time: 88.1 us -> 80.2 us (0.910)
  blocking collectives: 48.9 us -> 21.2 us
  starting transfers between devices: 4.26 us -> 16.4 us
  waiting for transfers between devices: 18.9 us -> 25.5 us
    all_to_all x2 -> x1, blocking collectives: 48.9 us -> 21.2 us  [exchange(): return lax.all_to_all(blocks, EP, 0, 0, tiled=True).reshape(block)]
    all_to_all x0 -> x1, waiting for transfers between devices: none -> 14.8 us  [exchange(): return lax.all_to_all(blocks, EP, 0, 0, tiled=True).reshape(block)]
    all_to_all x0 -> x1, starting transfers between devices: none -> 11.6 us  [exchange(): return lax.all_to_all(blocks, EP, 0, 0, tiled=True).reshape(block)]
    ppermute x3, waiting for transfers between devices: 17.6 us -> 9.45 us  [across(): return lax.ppermute(array, ('ep_0', 'ep_1', 'tp'), pairs)]
  transfers between devices with their start and end apart: 10 -> 11, of which waited for: 4 -> 4; matrix products, arithmetic and copies ran while one was open for 0% -> 0% of each run, Pallas kernels for 8% -> 9%
where the time goes in v2:
time: 80.2 us; the launch traced here: 80 us
  waiting for transfers between devices  25.5 us (32%)
  blocking collectives  21.2 us (26%)
  Pallas kernels  16.6 us (21%)
  starting transfers between devices  16.4 us (20%)
    all_to_all x1, blocking collectives, exchange(): return lax.all_to_all(blocks, EP, 0, 0, tiled=True).reshape(block)  21.2 us
    all_to_all x1, waiting for transfers between devices, exchange(): return lax.all_to_all(blocks, EP, 0, 0, tiled=True).reshape(block)  14.8 us
    all_to_all x1, starting transfers between devices, exchange(): return lax.all_to_all(blocks, EP, 0, 0, tiled=True).reshape(block)  11.6 us
    pallas_call x6, Pallas kernels, call(): pl.pallas_call(kernel, in_specs=[pl.BlockSpec(memory_space=space) for spa...  10.7 us
    ppermute x3, waiting for transfers between devices, across(): return lax.ppermute(array, ('ep_0', 'ep_1', 'tp'), pairs)  9.45 us
    pallas_call x1, Pallas kernels, attention(): pl.pallas_call(functools.partial(attention_kernel, peers=peers), in_specs...  5.95 us
    ppermute x3, starting transfers between devices, across(): return lax.ppermute(array, ('ep_0', 'ep_1', 'tp'), pairs)  3.68 us
  transfers between devices with their start and end apart: 11, of which 4 were waited for; matrix products, arithmetic and copies ran while one was open for 0% of the time, Pallas kernels for 9%

profile of v2, /device:TPU:0, one launch (start us, length us, event | category | flops | bytes accessed | tf_op | source)
XLA Modules:
  0.0 80.0 jit_solution(13520195657400373699)
XLA Ops:
  0.0 5.9 %attention.1 = (bf16[16,2048]{1,0:T(8,128)(2,1)S(1)}, bf16[16,384]{1,0:T(8,128)(2,1)S(1)}, bf16[32,384]{1,0:T(8,128)(2,1)S(1)}) custom-call(s32[16]{0:T(128)} %refs_0_.1, f32[4]{0:T(128)} %refs_1_.1, bf16[16,2048]{1,0:T(8,128)(2,1)} %tokens.1, f32[1,2048]{1,0:T(1,128)} %bitcast.27, bf16[2048,256]{1,0:T(8,128)(2,1)} %refs_4_.1, bf16[2048,256]{1,0:T(8,128)(2,1)} %refs_5_.1, ...), custom_call_target="tpu_custom_call" | custom-call | flops 184549376 | bytes 13631488 | tf_op jit(solution)/shard_map/attention/pallas_call | solution.py:195
  6.0 0.1 collective-permute-start
  6.1 1.2 %collective-permute-done.other = bf16[16,2048]{1,0:T(8,128)(2,1)S(1)} collective-permute-done((bf16[16,2048]{1,0:T(8,128)(2,1)S(1)}, bf16[16,2048]{1,0:T(8,128)(2,1)S(1)}, u32[]{:S(2)}, u32[]{:S(2)}) %collective-permute-start) | collective-permute-done | bytes 65568 | tf_op jit(solution)/shard_map/ppermute | solution.py:368
  7.3 1.7 %shard_map.235 = (bf16[3072,128]{1,0:T(8,128)(2,1)}, f32[16,1024]{1,0:T(8,128)S(1)}, f32[16,128]{1,0:T(8,128)S(1)}) custom-call(s32[1]{0:T(128)} %bitcast.8.core, bf16[16,2048]{1,0:T(8,128)(2,1)S(1)} %copy-done, bf16[16,2048]{1,0:T(8,128)(2,1)S(1)} %get-tuple-element.18.mine, bf16[16,2048]{1,0:T(8,128)(2,1)S(1)} %collective-permute-done.other, ...), custom_call_target="tpu_custom_call" | custom-call | flops 12582912 | bytes 1081348 | tf_op jit(solution)/shard_map/pallas_call | solution.py:262
  9.0 11.6 %all-to-all-start = ((bf16[64,48,128]{2,1,0:T(8,128)(2,1)}), bf16[64,48,128]{2,1,0:T(8,128)(2,1)S(1)}, u32[]{:S(2)}, u32[]{:S(2)}) async-start(bf16[64,48,128]{2,1,0:T(8,128)(2,1)} %bitcast.11), calls=%async_computation | async-start | bytes 1572864 | tf_op jit(solution)/shard_map/all_to_all | solution.py:416
  20.6 1.7 %collective-permute-start.2 = (bf16[96,2048]{1,0:T(8,128)(2,1)S(1)}, bf16[96,2048]{1,0:T(8,128)(2,1)S(1)}, u32[]{:S(2)}, u32[]{:S(2)}) collective-permute-start(bf16[96,2048]{1,0:T(8,128)(2,1)S(1)} %pad_maximum_fusion.refs_0_), channel_id=1, source_target_pairs={{0,32},{1,9},{8,40},{9,1},{16,48},{17,25},{24,56},{25,17},{32,0},{... | collective-permute-start | bytes 1179656 | tf_op jit(solution)/shard_map/ppermute | solution.py:379
  22.3 14.8 %all-to-all-done = bf16[64,48,128]{2,1,0:T(8,128)(2,1)S(1)} async-done(((bf16[64,48,128]{2,1,0:T(8,128)(2,1)}), bf16[64,48,128]{2,1,0:T(8,128)(2,1)S(1)}, u32[]{:S(2)}, u32[]{:S(2)}) %all-to-all-start) | async-done | bytes 786464 | tf_op jit(solution)/shard_map/all_to_all | solution.py:416
  37.1 0.0 collective-permute-start.1
  37.1 0.5 collective-permute-start.3
  37.6 0.0 collective-permute-done.2.refs_1_
  37.6 1.5 %collective-permute-start.4 = (bf16[96,2048]{1,0:T(8,128)(2,1)S(1)}, bf16[96,2048]{1,0:T(8,128)(2,1)S(1)}, u32[]{:S(2)}, u32[]{:S(2)}) collective-permute-start(bf16[96,2048]{1,0:T(8,128)(2,1)S(1)} %collective-permute-done.2.refs_1_), channel_id=1, source_target_pairs={{0,8},{1,33},{8,0},{9,41},{16,24},{17,49},{24,16},{25,57},{32,40},... | collective-permute-start | bytes 1179656 | tf_op jit(solution)/shard_map/ppermute | solution.py:379
  39.1 0.5 collective-permute-start.6
  39.6 5.2 %collective-permute-done.3.refs_2_ = bf16[96,2048]{1,0:T(8,128)(2,1)S(1)} collective-permute-done((bf16[96,2048]{1,0:T(8,128)(2,1)S(1)}, bf16[96,2048]{1,0:T(8,128)(2,1)S(1)}, u32[]{:S(2)}, u32[]{:S(2)}) %collective-permute-start.3) | collective-permute-done | bytes 393248 | tf_op jit(solution)/shard_map/ppermute | solution.py:379
  44.9 0.0 collective-permute-start.7
  44.9 4.2 %collective-permute-done.4.refs_3_ = bf16[96,2048]{1,0:T(8,128)(2,1)S(1)} collective-permute-done((bf16[96,2048]{1,0:T(8,128)(2,1)S(1)}, bf16[96,2048]{1,0:T(8,128)(2,1)S(1)}, u32[]{:S(2)}, u32[]{:S(2)}) %collective-permute-start.4) | collective-permute-done | bytes 393248 | tf_op jit(solution)/shard_map/ppermute | solution.py:379
  49.1 2.3 %shard_map.236 = (bf16[256,1024]{1,0:T(8,128)(2,1)S(1)}, f32[128,768]{1,0:T(8,128)S(1)}, f32[128,768]{1,0:T(8,128)S(1)}) custom-call(s32[1]{0:T(128)} %bitcast.8.core, bf16[3072,128]{1,0:T(8,128)(2,1)S(1)} %bitcast.18, bf16[1,2048,768]{2,1,0:T(8,128)(2,1)} %gate_far.3, bf16[1,2048,768]{2,1,0:T(8,128)(2,1)} %up_far.3), custom_call_target="tpu_custom_call" | custom-call | flops 402653184 | bytes 8388612 | tf_op jit(solution)/shard_map/pallas_call | solution.py:262
  51.5 0.0 collective-permute-done.1.other
  51.5 3.5 %shard_map.237 = (bf16[256,1024]{1,0:T(8,128)(2,1)S(1)}, bf16[128,1024]{1,0:T(8,128)(2,1)S(1)}, bf16[128,1024]{1,0:T(8,128)(2,1)S(1)}) custom-call(s32[1]{0:T(128)} %bitcast.8.core, bf16[3072,128]{1,0:T(8,128)(2,1)S(1)} %collective-permute-done.1.other, f32[128,768]{1,0:T(8,128)S(1)} %get-tuple-element.22.gate_part, ...), custom_call_target="tpu_custom_call" | custom-call | flops 805306368 | bytes 12058628 | tf_op jit(solution)/shard_map/pallas_call | solution.py:262
  55.0 0.6 collective-permute-start.9
  55.6 1.1 %shard_map.238.dense = f32[256,1024]{1,0:T(8,128)S(1)} custom-call(s32[1]{0:T(128)} %bitcast.8.core, bf16[256,1024]{1,0:T(8,128)(2,1)S(1)} %get-tuple-element.21.mine, bf16[256,1024]{1,0:T(8,128)(2,1)S(1)} %get-tuple-element.24.other, bf16[96,2048]{1,0:T(8,128)(2,1)S(1)} %pad_maximum_fusion.refs_0_, bf16[96,2048]{1,0:T(8,128)(2,1)S(1)} %collective-permute-done.2.refs_1_, ...), custom_call_target="tpu_custom_call" | custom-call | flops 671088640 | bytes 5242884 | tf_op jit(solution)/shard_map/pallas_call | solution.py:262
  56.7 0.0 collective-permute-done.9.other
  56.7 0.6 shard_map.239
  57.3 21.2 %all_to_all.10 = bf16[64,48,128]{2,1,0:T(8,128)(2,1)S(1)} all-to-all(bf16[64,48,128]{2,1,0:T(8,128)(2,1)S(1)} %bitcast.20), channel_id=1, replica_groups=mesh['ep_0'=4,'ep_1'=4,'ep_2'=4,'tp'=2] {'ep_0','ep_1','ep_2'}, dimensions={0} | all-to-all | bytes 1572864 | tf_op jit(solution)/shard_map/all_to_all | solution.py:416
  78.5 1.5 %shard_map.240 = bf16[16,1024]{1,0:T(8,128)(2,1)} custom-call(bf16[32,384]{1,0:T(8,128)(2,1)S(1)} %get-tuple-element.17.home_map, bf16[3072,128]{1,0:T(8,128)(2,1)S(1)} %bitcast.19, f32[16,1024]{1,0:T(8,128)S(1)} %get-tuple-element.27.kept, f32[16,128]{1,0:T(8,128)S(1)} %get-tuple-element.28.row_gate), custom_call_target="tpu_custom_call" | custom-call | flops 25165824 | bytes 917504 | tf_op jit(solution)/shard_map/pallas_call | solution.py:262
  (19 shorter events, 0.1 us)
Async XLA Ops:
  0.0 7.3 %copy-start = (bf16[16,2048]{1,0:T(8,128)(2,1)S(1)}, bf16[16,2048]{1,0:T(8,128)(2,1)}, u32[]{:S(2)}) copy-start(bf16[16,2048]{1,0:T(8,128)(2,1)} %tokens.1) | copy-start | bytes 196612
  0.0 7.3 %copy-start.1 = (f32[2048]{0:T(1024)S(1)}, f32[2048]{0:T(1024)}, u32[]{:S(2)}) copy-start(f32[2048]{0:T(1024)} %param.40) | copy-start | bytes 24580
  0.0 7.3 %copy-start.2 = (bf16[2048]{0:T(1024)(128)(2,1)S(1)}, bf16[2048]{0:T(1024)(128)(2,1)}, u32[]{:S(2)}) copy-start(bf16[2048]{0:T(1024)(128)(2,1)} %param.46) | copy-start | bytes 12292
  0.0 20.6 %copy-start.3 = (bf16[32,2048]{1,0:T(8,128)(2,1)S(1)}, bf16[32,2048]{1,0:T(8,128)(2,1)}, u32[]{:S(2)}) copy-start(bf16[32,2048]{1,0:T(8,128)(2,1)} %param.49) | copy-start | bytes 393220
  0.0 20.6 %copy-start.4 = (bf16[2048,32]{0,1:T(8,128)(2,1)S(1)}, bf16[2048,32]{0,1:T(8,128)(2,1)}, u32[]{:S(2)}) copy-start(bf16[2048,32]{0,1:T(8,128)(2,1)} %param.48) | copy-start | bytes 393220
  0.0 20.6 %copy-start.5 = (bf16[2048,32]{0,1:T(8,128)(2,1)S(1)}, bf16[2048,32]{0,1:T(8,128)(2,1)}, u32[]{:S(2)}) copy-start(bf16[2048,32]{0,1:T(8,128)(2,1)} %param.47) | copy-start | bytes 393220
  6.0 1.3 %collective-permute-start = (bf16[16,2048]{1,0:T(8,128)(2,1)S(1)}, bf16[16,2048]{1,0:T(8,128)(2,1)S(1)}, u32[]{:S(2)}, u32[]{:S(2)}) collective-permute-start(bf16[16,2048]{1,0:T(8,128)(2,1)S(1)} %get-tuple-element.18.mine), channel_id=1, source_target_pairs={{0,1},{1,0},{2,3},{3,2},{4,5},{5,4},{6,7},{7,6},{8,9},{9,8},{10,11... | collective-permute-start | bytes 196616 | tf_op jit(solution)/shard_map/ppermute | solution.py:368
  9.0 28.1 %all-to-all-start = ((bf16[64,48,128]{2,1,0:T(8,128)(2,1)}), bf16[64,48,128]{2,1,0:T(8,128)(2,1)S(1)}, u32[]{:S(2)}, u32[]{:S(2)}) async-start(bf16[64,48,128]{2,1,0:T(8,128)(2,1)} %bitcast.11), calls=%async_computation | async-start | bytes 1572864 | tf_op jit(solution)/shard_map/all_to_all | solution.py:416
  20.6 17.0 %collective-permute-start.2 = (bf16[96,2048]{1,0:T(8,128)(2,1)S(1)}, bf16[96,2048]{1,0:T(8,128)(2,1)S(1)}, u32[]{:S(2)}, u32[]{:S(2)}) collective-permute-start(bf16[96,2048]{1,0:T(8,128)(2,1)S(1)} %pad_maximum_fusion.refs_0_), channel_id=1, source_target_pairs={{0,32},{1,9},{8,40},{9,1},{16,48},{17,25},{24,56},{25,17},{32,0},{... | collective-permute-start | bytes 1179656 | tf_op jit(solution)/shard_map/ppermute | solution.py:379
  37.1 14.3 %collective-permute-start.1 = (bf16[3072,128]{1,0:T(8,128)(2,1)S(1)}, bf16[3072,128]{1,0:T(8,128)(2,1)S(1)}, u32[]{:S(2)}, u32[]{:S(2)}) collective-permute-start(bf16[3072,128]{1,0:T(8,128)(2,1)S(1)} %bitcast.17), channel_id=1, source_target_pairs={{0,1},{1,0},{2,3},{3,2},{4,5},{5,4},{6,7},{7,6},{8,9},{9,8},{10,11... | collective-permute-start | bytes 2359304 | tf_op jit(solution)/shard_map/ppermute | solution.py:368
  37.1 7.8 %collective-permute-start.3 = (bf16[96,2048]{1,0:T(8,128)(2,1)S(1)}, bf16[96,2048]{1,0:T(8,128)(2,1)S(1)}, u32[]{:S(2)}, u32[]{:S(2)}) collective-permute-start(bf16[96,2048]{1,0:T(8,128)(2,1)S(1)} %pad_maximum_fusion.refs_0_), channel_id=1, source_target_pairs={{0,8},{1,33},{8,0},{9,41},{16,24},{17,49},{24,16},{25,57},{32,40},... | collective-permute-start | bytes 1179656 | tf_op jit(solution)/shard_map/ppermute | solution.py:379
  37.6 11.5 %collective-permute-start.4 = (bf16[96,2048]{1,0:T(8,128)(2,1)S(1)}, bf16[96,2048]{1,0:T(8,128)(2,1)S(1)}, u32[]{:S(2)}, u32[]{:S(2)}) collective-permute-start(bf16[96,2048]{1,0:T(8,128)(2,1)S(1)} %collective-permute-done.2.refs_1_), channel_id=1, source_target_pairs={{0,8},{1,33},{8,0},{9,41},{16,24},{17,49},{24,16},{25,57},{32,40},... | collective-permute-start | bytes 1179656 | tf_op jit(solution)/shard_map/ppermute | solution.py:379
  39.1 16.4 %collective-permute-start.5 = (bf16[96,2048]{1,0:T(8,128)(2,1)S(1)}, bf16[96,2048]{1,0:T(8,128)(2,1)S(1)}, u32[]{:S(2)}, u32[]{:S(2)}) collective-permute-start(bf16[96,2048]{1,0:T(8,128)(2,1)S(1)} %pad_maximum_fusion.refs_0_), channel_id=1, source_target_pairs={{0,1},{1,0},{2,3},{3,2},{4,5},{5,4},{6,7},{7,6},{8,9},{9,8},{10,11... | collective-permute-start | bytes 1179656 | tf_op jit(solution)/shard_map/ppermute | solution.py:368
  39.1 16.4 %collective-permute-start.6 = (bf16[96,2048]{1,0:T(8,128)(2,1)S(1)}, bf16[96,2048]{1,0:T(8,128)(2,1)S(1)}, u32[]{:S(2)}, u32[]{:S(2)}) collective-permute-start(bf16[96,2048]{1,0:T(8,128)(2,1)S(1)} %collective-permute-done.2.refs_1_), channel_id=1, source_target_pairs={{0,1},{1,0},{2,3},{3,2},{4,5},{5,4},{6,7},{7,6},{8,9},{9,8},{10,11... | collective-permute-start | bytes 1179656 | tf_op jit(solution)/shard_map/ppermute | solution.py:368
  44.9 10.7 %collective-permute-start.7 = (bf16[96,2048]{1,0:T(8,128)(2,1)S(1)}, bf16[96,2048]{1,0:T(8,128)(2,1)S(1)}, u32[]{:S(2)}, u32[]{:S(2)}) collective-permute-start(bf16[96,2048]{1,0:T(8,128)(2,1)S(1)} %collective-permute-done.3.refs_2_), channel_id=1, source_target_pairs={{0,1},{1,0},{2,3},{3,2},{4,5},{5,4},{6,7},{7,6},{8,9},{9,8},{10,11... | collective-permute-start | bytes 1179656 | tf_op jit(solution)/shard_map/ppermute | solution.py:368
  49.1 6.5 %collective-permute-start.8 = (bf16[96,2048]{1,0:T(8,128)(2,1)S(1)}, bf16[96,2048]{1,0:T(8,128)(2,1)S(1)}, u32[]{:S(2)}, u32[]{:S(2)}) collective-permute-start(bf16[96,2048]{1,0:T(8,128)(2,1)S(1)} %collective-permute-done.4.refs_3_), channel_id=1, source_target_pairs={{0,1},{1,0},{2,3},{3,2},{4,5},{5,4},{6,7},{7,6},{8,9},{9,8},{10,11... | collective-permute-start | bytes 1179656 | tf_op jit(solution)/shard_map/ppermute | solution.py:368
  55.0 1.8 %collective-permute-start.9 = (bf16[128,1024]{1,0:T(8,128)(2,1)S(1)}, bf16[128,1024]{1,0:T(8,128)(2,1)S(1)}, u32[]{:S(2)}, u32[]{:S(2)}) collective-permute-start(bf16[128,1024]{1,0:T(8,128)(2,1)S(1)} %get-tuple-element.26), channel_id=1, source_target_pairs={{0,1},{1,0},{2,3},{3,2},{4,5},{5,4},{6,7},{7,6},{8,9},{9,8},{10,11... | collective-permute-start | bytes 786440 | tf_op jit(solution)/shard_map/ppermute | solution.py:368

commit v3 on v2

--- a/solution.py
+++ b/solution.py
@@ -250,7 +250,7 @@
     send[...] = wide_s[...].astype(bf16)
 
 
-def call(kernel, args, outs, scratch, flops, transcendentals=0, far=0):
+def call(kernel, args, outs, scratch, flops, transcendentals=0, far=0, sems=0):
     near = len(args) - far
     spaces = [pltpu.SMEM if one.ndim == 1 else pltpu.VMEM for one in args[:near]]
     spaces += [pltpu.HBM] * far
@@ -265,7 +265,7 @@
         out_specs=[pl.BlockSpec(memory_space=pltpu.VMEM)] * len(outs),
         out_shape=out_shape,
         scratch_shapes=[pltpu.VMEM(*one) for one in scratch]
-        + [pltpu.SemaphoreType.DMA((far,))] * (far > 0),
+        + [pltpu.SemaphoreType.DMA((sems,))] * (sems > 0),
         compiler_params=pltpu.CompilerParams(vmem_limit_bytes=LIMIT // 2),
         cost_estimate=pl.CostEstimate(
             flops=flops, bytes_accessed=moved, transcendentals=transcendentals
@@ -284,44 +284,43 @@
 
 
 def first_kernel(
-    core, mine, gate_far, up_far, rows_d, gate_part, up_part, wide_s, rows_e, gate, up, sems
+    core, mine, gate_far, up_far, rows_d, gate_part, up_part, gate_back, up_back,
+    wide_s, rows_e, gate, up, sems,
 ):
     half = rows_d.shape[1]
     own = pl.ds(pl.multiple_of(core[0] * half, half), half)
+    back = pl.ds(pl.multiple_of((1 - core[0]) * half, half), half)
     fetch_gate = pltpu.make_async_copy(gate_far.at[0, own], gate, sems.at[0])
     fetch_up = pltpu.make_async_copy(up_far.at[0, own], up, sems.at[1])
-    fetch_gate.start()
-    fetch_up.start()
+    later = [
+        pltpu.make_async_copy(gate_far.at[0, back], gate_back, sems.at[2]),
+        pltpu.make_async_copy(up_far.at[0, back], up_back, sems.at[3]),
+    ]
+    for one in [fetch_gate, fetch_up] + later:
+        one.start()
     wide_s[...] = mine[...].astype(f32)
     compact(wide_s, rows_e, rows_d)
     fetch_gate.wait()
     gate_part[...] = mm(rows_e[...], gate[...])
     fetch_up.wait()
     up_part[...] = mm(rows_e[...], up[...])
+    for one in later:
+        one.wait()
 
 
 def second_kernel(
-    core, other, gate_part, up_part, gate_far, up_far, down_far, rows_d, out_mine, out_other,
-    wide_s, rows_e, total, gate, up, down, sems,
+    core, other, gate_part, up_part, gate, up, down, rows_d, out_mine, out_other,
+    wide_s, rows_e, total,
 ):
     half = rows_d.shape[1]
     at = pl.multiple_of(core[0] * half, half)
     back = pl.multiple_of((1 - core[0]) * half, half)
-    fetch_gate = pltpu.make_async_copy(gate_far.at[0, pl.ds(back, half)], gate, sems.at[0])
-    fetch_up = pltpu.make_async_copy(up_far.at[0, pl.ds(back, half)], up, sems.at[1])
-    fetch_down = pltpu.make_async_copy(down_far.at[0], down, sems.at[2])
-    fetch_gate.start()
-    fetch_up.start()
-    fetch_down.start()
     wide_s[...] = other[...].astype(f32)
     compact(wide_s, rows_e, rows_d)
-    fetch_gate.wait()
     gate_pre = gate_part[...] + mm(rows_e[...], gate[...])
-    fetch_up.wait()
     up_pre = up_part[...] + mm(rows_e[...], up[...])
     hidden = clamped_unit(gate_pre, up_pre).astype(bf16)
-    fetch_down.wait()
-    total[...] = mm(hidden, down[...])
+    total[...] = mm(hidden, down[0])
     out_mine[...] = total[:, pl.ds(at, half)].astype(bf16)
     out_other[...] = total[:, pl.ds(back, half)].astype(bf16)
 
@@ -417,24 +416,24 @@
 
     mine = exchange(send)
     other = swap(mine)
-    rows_mine, gate_part, up_part = call(
+    rows_mine, gate_part, up_part, gate_back, up_back = call(
         first_kernel,
         (core, mine, expert_gate, expert_up),
-        [((DENSE_ROWS * peers, half), bf16)] + [((slots, hidden), f32)] * 2,
+        [((DENSE_ROWS * peers, half), bf16)]
+        + [((slots, hidden), f32)] * 2
+        + [((half, hidden), bf16)] * 2,
         [(block, f32), ((slots, half), bf16)] + [((half, hidden), bf16)] * 2,
         4 * slots * half * hidden,
         far=2,
+        sems=4,
     )
     rows_other, own, sent = call(
         second_kernel,
-        (core, other, gate_part, up_part, expert_gate, expert_up, expert_down),
+        (core, other, gate_part, up_part, gate_back, up_back, expert_down),
         [((DENSE_ROWS * peers, half), bf16)] + [((slots, half), bf16)] * 2,
-        [(block, f32), ((slots, half), bf16), ((slots, width), f32)]
-        + [((half, hidden), bf16)] * 2
-        + [((hidden, width), bf16)],
+        [(block, f32), ((slots, half), bf16), ((slots, width), f32)],
         8 * slots * half * hidden,
         slots * hidden,
-        far=3,
     )
     came = swap(sent)
     packs = [pack, pack0, pack1, pack2]

time: 80.2 us -> 79 us (0.985)
  Pallas kernels: 16.6 us -> 15.4 us
    pallas_call x6, Pallas kernels: 10.7 us -> 9.42 us  [call(): pl.pallas_call(kernel, in_specs=[pl.BlockSpec(memory_space=space) for spa...]
  transfers between devices with their start and end apart: 11 -> 11, of which waited for: 4 -> 4; matrix products, arithmetic and copies ran while one was open for 0% -> 0% of each run, Pallas kernels for 9% -> 7%
where the time goes in v3:
time: 79 us; the launch traced here: 78.8 us
  waiting for transfers between devices  25.5 us (32%)
  blocking collectives  21.2 us (27%)
  starting transfers between devices  16.4 us (21%)
  Pallas kernels  15.4 us (19%)
    all_to_all x1, blocking collectives, exchange(): return lax.all_to_all(blocks, EP, 0, 0, tiled=True).reshape(block)  21.2 us
    all_to_all x1, waiting for transfers between devices, exchange(): return lax.all_to_all(blocks, EP, 0, 0, tiled=True).reshape(block)  14.8 us
    all_to_all x1, starting transfers between devices, exchange(): return lax.all_to_all(blocks, EP, 0, 0, tiled=True).reshape(block)  11.6 us
    ppermute x3, waiting for transfers between devices, across(): return lax.ppermute(array, ('ep_0', 'ep_1', 'tp'), pairs)  9.45 us
    pallas_call x6, Pallas kernels, call(): pl.pallas_call(kernel, in_specs=[pl.BlockSpec(memory_space=space) for spa...  9.42 us
    pallas_call x1, Pallas kernels, attention(): pl.pallas_call(functools.partial(attention_kernel, peers=peers), in_specs...  5.95 us
    ppermute x3, starting transfers between devices, across(): return lax.ppermute(array, ('ep_0', 'ep_1', 'tp'), pairs)  3.68 us
  transfers between devices with their start and end apart: 11, of which 4 were waited for; matrix products, arithmetic and copies ran while one was open for 0% of the time, Pallas kernels for 7%

profile of v3, /device:TPU:0, one launch (start us, length us, event | category | flops | bytes accessed | tf_op | source)
XLA Modules:
  0.0 78.8 jit_solution(17404084742486085697)
XLA Ops:
  0.0 5.9 %attention.1 = (bf16[16,2048]{1,0:T(8,128)(2,1)S(1)}, bf16[16,384]{1,0:T(8,128)(2,1)S(1)}, bf16[32,384]{1,0:T(8,128)(2,1)S(1)}) custom-call(s32[16]{0:T(128)} %refs_0_.1, f32[4]{0:T(128)} %refs_1_.1, bf16[16,2048]{1,0:T(8,128)(2,1)} %tokens.1, f32[1,2048]{1,0:T(1,128)} %bitcast.27, bf16[2048,256]{1,0:T(8,128)(2,1)} %refs_4_.1, bf16[2048,256]{1,0:T(8,128)(2,1)} %refs_5_.1, ...), custom_call_target="tpu_custom_call" | custom-call | flops 184549376 | bytes 13631488 | tf_op jit(solution)/shard_map/attention/pallas_call | solution.py:195
  6.0 0.1 collective-permute-start
  6.1 1.2 %collective-permute-done.other = bf16[16,2048]{1,0:T(8,128)(2,1)S(1)} collective-permute-done((bf16[16,2048]{1,0:T(8,128)(2,1)S(1)}, bf16[16,2048]{1,0:T(8,128)(2,1)S(1)}, u32[]{:S(2)}, u32[]{:S(2)}) %collective-permute-start) | collective-permute-done | bytes 65568 | tf_op jit(solution)/shard_map/ppermute | solution.py:367
  7.3 1.7 %shard_map.235 = (bf16[3072,128]{1,0:T(8,128)(2,1)}, f32[16,1024]{1,0:T(8,128)S(1)}, f32[16,128]{1,0:T(8,128)S(1)}) custom-call(s32[1]{0:T(128)} %bitcast.8.core, bf16[16,2048]{1,0:T(8,128)(2,1)S(1)} %copy-done.1, bf16[16,2048]{1,0:T(8,128)(2,1)S(1)} %get-tuple-element.20.mine, bf16[16,2048]{1,0:T(8,128)(2,1)S(1)} %collective-permute-done.other, ...), custom_call_target="tpu_custom_call" | custom-call | flops 12582912 | bytes 1081348 | tf_op jit(solution)/shard_map/pallas_call | solution.py:262
  9.0 11.6 %all-to-all-start = ((bf16[64,48,128]{2,1,0:T(8,128)(2,1)}), bf16[64,48,128]{2,1,0:T(8,128)(2,1)S(1)}, u32[]{:S(2)}, u32[]{:S(2)}) async-start(bf16[64,48,128]{2,1,0:T(8,128)(2,1)} %bitcast.11), calls=%async_computation | async-start | bytes 1572864 | tf_op jit(solution)/shard_map/all_to_all | solution.py:415
  20.6 1.7 %collective-permute-start.2 = (bf16[96,2048]{1,0:T(8,128)(2,1)S(1)}, bf16[96,2048]{1,0:T(8,128)(2,1)S(1)}, u32[]{:S(2)}, u32[]{:S(2)}) collective-permute-start(bf16[96,2048]{1,0:T(8,128)(2,1)S(1)} %pad_maximum_fusion.refs_0_), channel_id=1, source_target_pairs={{0,32},{1,9},{8,40},{9,1},{16,48},{17,25},{24,56},{25,17},{32,0},{... | collective-permute-start | bytes 1179656 | tf_op jit(solution)/shard_map/ppermute | solution.py:378
  22.3 14.8 %all-to-all-done = bf16[64,48,128]{2,1,0:T(8,128)(2,1)S(1)} async-done(((bf16[64,48,128]{2,1,0:T(8,128)(2,1)}), bf16[64,48,128]{2,1,0:T(8,128)(2,1)S(1)}, u32[]{:S(2)}, u32[]{:S(2)}) %all-to-all-start) | async-done | bytes 786464 | tf_op jit(solution)/shard_map/all_to_all | solution.py:415
  37.1 0.5 collective-permute-start.3
  37.6 1.5 %collective-permute-start.4 = (bf16[96,2048]{1,0:T(8,128)(2,1)S(1)}, bf16[96,2048]{1,0:T(8,128)(2,1)S(1)}, u32[]{:S(2)}, u32[]{:S(2)}) collective-permute-start(bf16[96,2048]{1,0:T(8,128)(2,1)S(1)} %collective-permute-done.2.refs_1_), channel_id=1, source_target_pairs={{0,8},{1,33},{8,0},{9,41},{16,24},{17,49},{24,16},{25,57},{32,40},... | collective-permute-start | bytes 1179656 | tf_op jit(solution)/shard_map/ppermute | solution.py:378
  39.2 0.0 collective-permute-start.5
  39.2 0.5 collective-permute-start.6
  39.7 5.2 %collective-permute-done.3.refs_2_ = bf16[96,2048]{1,0:T(8,128)(2,1)S(1)} collective-permute-done((bf16[96,2048]{1,0:T(8,128)(2,1)S(1)}, bf16[96,2048]{1,0:T(8,128)(2,1)S(1)}, u32[]{:S(2)}, u32[]{:S(2)}) %collective-permute-start.3) | collective-permute-done | bytes 393248 | tf_op jit(solution)/shard_map/ppermute | solution.py:378
  44.9 0.0 collective-permute-start.7
  44.9 4.2 %collective-permute-done.4.refs_3_ = bf16[96,2048]{1,0:T(8,128)(2,1)S(1)} collective-permute-done((bf16[96,2048]{1,0:T(8,128)(2,1)S(1)}, bf16[96,2048]{1,0:T(8,128)(2,1)S(1)}, u32[]{:S(2)}, u32[]{:S(2)}) %collective-permute-start.4) | collective-permute-done | bytes 393248 | tf_op jit(solution)/shard_map/ppermute | solution.py:378
  49.1 0.0 collective-permute-start.8
  49.1 2.9 %shard_map.236 = (bf16[256,1024]{1,0:T(8,128)(2,1)S(1)}, f32[128,768]{1,0:T(8,128)S(1)}, f32[128,768]{1,0:T(8,128)S(1)}, bf16[1024,768]{1,0:T(8,128)(2,1)S(1)}, bf16[1024,768]{1,0:T(8,128)(2,1)S(1)}) custom-call(s32[1]{0:T(128)} %bitcast.8.core, bf16[3072,128]{1,0:T(8,128)(2,1)S(1)} %bitcast.18, bf16[1,2048,768]{2,1,0:T(8,128)(2,1)} %gate_far.1, ...), custom_call_target="tpu_custom_call" | custom-call | flops 402653184 | bytes 11534340 | tf_op jit(solution)/shard_map/pallas_call | solution.py:262
  52.0 0.0 collective-permute-done.1.other
  52.0 1.7 %shard_map.237 = (bf16[256,1024]{1,0:T(8,128)(2,1)S(1)}, bf16[128,1024]{1,0:T(8,128)(2,1)S(1)}, bf16[128,1024]{1,0:T(8,128)(2,1)S(1)}) custom-call(s32[1]{0:T(128)} %bitcast.8.core, bf16[3072,128]{1,0:T(8,128)(2,1)S(1)} %collective-permute-done.1.other, f32[128,768]{1,0:T(8,128)S(1)} %get-tuple-element.24.gate_part, ...), custom_call_target="tpu_custom_call" | custom-call | flops 805306368 | bytes 8912900 | tf_op jit(solution)/shard_map/pallas_call | solution.py:262
  53.8 0.6 collective-permute-start.9
  54.4 1.1 %shard_map.238.dense = f32[256,1024]{1,0:T(8,128)S(1)} custom-call(s32[1]{0:T(128)} %bitcast.8.core, bf16[256,1024]{1,0:T(8,128)(2,1)S(1)} %get-tuple-element.23.mine, bf16[256,1024]{1,0:T(8,128)(2,1)S(1)} %get-tuple-element.28.other, bf16[96,2048]{1,0:T(8,128)(2,1)S(1)} %pad_maximum_fusion.refs_0_, bf16[96,2048]{1,0:T(8,128)(2,1)S(1)} %collective-permute-done.2.refs_1_, ...), custom_call_target="tpu_custom_call" | custom-call | flops 671088640 | bytes 5242884 | tf_op jit(solution)/shard_map/pallas_call | solution.py:262
  55.5 0.0 collective-permute-done.9.other
  55.5 0.6 shard_map.239
  56.1 21.2 %all_to_all.10 = bf16[64,48,128]{2,1,0:T(8,128)(2,1)S(1)} all-to-all(bf16[64,48,128]{2,1,0:T(8,128)(2,1)S(1)} %bitcast.20), channel_id=1, replica_groups=mesh['ep_0'=4,'ep_1'=4,'ep_2'=4,'tp'=2] {'ep_0','ep_1','ep_2'}, dimensions={0} | all-to-all | bytes 1572864 | tf_op jit(solution)/shard_map/all_to_all | solution.py:415
  77.3 1.5 %shard_map.240 = bf16[16,1024]{1,0:T(8,128)(2,1)} custom-call(bf16[32,384]{1,0:T(8,128)(2,1)S(1)} %get-tuple-element.19.home_map, bf16[3072,128]{1,0:T(8,128)(2,1)S(1)} %bitcast.19, f32[16,1024]{1,0:T(8,128)S(1)} %get-tuple-element.31.kept, f32[16,128]{1,0:T(8,128)S(1)} %get-tuple-element.32.row_gate), custom_call_target="tpu_custom_call" | custom-call | flops 25165824 | bytes 917504 | tf_op jit(solution)/shard_map/pallas_call | solution.py:262
  (21 shorter events, 0.1 us)
Async XLA Ops:
  0.0 7.3 %copy-start.1 = (bf16[16,2048]{1,0:T(8,128)(2,1)S(1)}, bf16[16,2048]{1,0:T(8,128)(2,1)}, u32[]{:S(2)}) copy-start(bf16[16,2048]{1,0:T(8,128)(2,1)} %tokens.1) | copy-start | bytes 196612
  0.0 7.3 %copy-start.2 = (f32[2048]{0:T(1024)S(1)}, f32[2048]{0:T(1024)}, u32[]{:S(2)}) copy-start(f32[2048]{0:T(1024)} %param.40) | copy-start | bytes 24580
  0.0 7.3 %copy-start.3 = (bf16[2048]{0:T(1024)(128)(2,1)S(1)}, bf16[2048]{0:T(1024)(128)(2,1)}, u32[]{:S(2)}) copy-start(bf16[2048]{0:T(1024)(128)(2,1)} %param.46) | copy-start | bytes 12292
  0.0 20.6 %copy-start.4 = (bf16[32,2048]{1,0:T(8,128)(2,1)S(1)}, bf16[32,2048]{1,0:T(8,128)(2,1)}, u32[]{:S(2)}) copy-start(bf16[32,2048]{1,0:T(8,128)(2,1)} %param.49) | copy-start | bytes 393220
  0.0 20.6 %copy-start.5 = (bf16[2048,32]{0,1:T(8,128)(2,1)S(1)}, bf16[2048,32]{0,1:T(8,128)(2,1)}, u32[]{:S(2)}) copy-start(bf16[2048,32]{0,1:T(8,128)(2,1)} %param.48) | copy-start | bytes 393220
  0.0 20.6 %copy-start.6 = (bf16[2048,32]{0,1:T(8,128)(2,1)S(1)}, bf16[2048,32]{0,1:T(8,128)(2,1)}, u32[]{:S(2)}) copy-start(bf16[2048,32]{0,1:T(8,128)(2,1)} %param.47) | copy-start | bytes 393220
  6.0 1.3 %collective-permute-start = (bf16[16,2048]{1,0:T(8,128)(2,1)S(1)}, bf16[16,2048]{1,0:T(8,128)(2,1)S(1)}, u32[]{:S(2)}, u32[]{:S(2)}) collective-permute-start(bf16[16,2048]{1,0:T(8,128)(2,1)S(1)} %get-tuple-element.20.mine), channel_id=1, source_target_pairs={{0,1},{1,0},{2,3},{3,2},{4,5},{5,4},{6,7},{7,6},{8,9},{9,8},{10,11... | collective-permute-start | bytes 196616 | tf_op jit(solution)/shard_map/ppermute | solution.py:367
  9.0 28.1 %all-to-all-start = ((bf16[64,48,128]{2,1,0:T(8,128)(2,1)}), bf16[64,48,128]{2,1,0:T(8,128)(2,1)S(1)}, u32[]{:S(2)}, u32[]{:S(2)}) async-start(bf16[64,48,128]{2,1,0:T(8,128)(2,1)} %bitcast.11), calls=%async_computation | async-start | bytes 1572864 | tf_op jit(solution)/shard_map/all_to_all | solution.py:415
  20.6 17.0 %collective-permute-start.2 = (bf16[96,2048]{1,0:T(8,128)(2,1)S(1)}, bf16[96,2048]{1,0:T(8,128)(2,1)S(1)}, u32[]{:S(2)}, u32[]{:S(2)}) collective-permute-start(bf16[96,2048]{1,0:T(8,128)(2,1)S(1)} %pad_maximum_fusion.refs_0_), channel_id=1, source_target_pairs={{0,32},{1,9},{8,40},{9,1},{16,48},{17,25},{24,56},{25,17},{32,0},{... | collective-permute-start | bytes 1179656 | tf_op jit(solution)/shard_map/ppermute | solution.py:378
  37.1 14.9 %copy-start = (bf16[1,768,2048]{2,1,0:T(8,128)(2,1)S(1)}, bf16[1,768,2048]{2,1,0:T(8,128)(2,1)}, u32[]{:S(2)}) copy-start(bf16[1,768,2048]{2,1,0:T(8,128)(2,1)} %down.1) | copy-start | bytes 9437188
  37.1 14.9 %collective-permute-start.1 = (bf16[3072,128]{1,0:T(8,128)(2,1)S(1)}, bf16[3072,128]{1,0:T(8,128)(2,1)S(1)}, u32[]{:S(2)}, u32[]{:S(2)}) collective-permute-start(bf16[3072,128]{1,0:T(8,128)(2,1)S(1)} %bitcast.17), channel_id=1, source_target_pairs={{0,1},{1,0},{2,3},{3,2},{4,5},{5,4},{6,7},{7,6},{8,9},{9,8},{10,11... | collective-permute-start | bytes 2359304 | tf_op jit(solution)/shard_map/ppermute | solution.py:367
  37.1 7.8 %collective-permute-start.3 = (bf16[96,2048]{1,0:T(8,128)(2,1)S(1)}, bf16[96,2048]{1,0:T(8,128)(2,1)S(1)}, u32[]{:S(2)}, u32[]{:S(2)}) collective-permute-start(bf16[96,2048]{1,0:T(8,128)(2,1)S(1)} %pad_maximum_fusion.refs_0_), channel_id=1, source_target_pairs={{0,8},{1,33},{8,0},{9,41},{16,24},{17,49},{24,16},{25,57},{32,40},... | collective-permute-start | bytes 1179656 | tf_op jit(solution)/shard_map/ppermute | solution.py:378
  37.6 11.5 %collective-permute-start.4 = (bf16[96,2048]{1,0:T(8,128)(2,1)S(1)}, bf16[96,2048]{1,0:T(8,128)(2,1)S(1)}, u32[]{:S(2)}, u32[]{:S(2)}) collective-permute-start(bf16[96,2048]{1,0:T(8,128)(2,1)S(1)} %collective-permute-done.2.refs_1_), channel_id=1, source_target_pairs={{0,8},{1,33},{8,0},{9,41},{16,24},{17,49},{24,16},{25,57},{32,40},... | collective-permute-start | bytes 1179656 | tf_op jit(solution)/shard_map/ppermute | solution.py:378
  39.2 15.2 %collective-permute-start.5 = (bf16[96,2048]{1,0:T(8,128)(2,1)S(1)}, bf16[96,2048]{1,0:T(8,128)(2,1)S(1)}, u32[]{:S(2)}, u32[]{:S(2)}) collective-permute-start(bf16[96,2048]{1,0:T(8,128)(2,1)S(1)} %pad_maximum_fusion.refs_0_), channel_id=1, source_target_pairs={{0,1},{1,0},{2,3},{3,2},{4,5},{5,4},{6,7},{7,6},{8,9},{9,8},{10,11... | collective-permute-start | bytes 1179656 | tf_op jit(solution)/shard_map/ppermute | solution.py:367
  39.2 15.2 %collective-permute-start.6 = (bf16[96,2048]{1,0:T(8,128)(2,1)S(1)}, bf16[96,2048]{1,0:T(8,128)(2,1)S(1)}, u32[]{:S(2)}, u32[]{:S(2)}) collective-permute-start(bf16[96,2048]{1,0:T(8,128)(2,1)S(1)} %collective-permute-done.2.refs_1_), channel_id=1, source_target_pairs={{0,1},{1,0},{2,3},{3,2},{4,5},{5,4},{6,7},{7,6},{8,9},{9,8},{10,11... | collective-permute-start | bytes 1179656 | tf_op jit(solution)/shard_map/ppermute | solution.py:367
  44.9 9.5 %collective-permute-start.7 = (bf16[96,2048]{1,0:T(8,128)(2,1)S(1)}, bf16[96,2048]{1,0:T(8,128)(2,1)S(1)}, u32[]{:S(2)}, u32[]{:S(2)}) collective-permute-start(bf16[96,2048]{1,0:T(8,128)(2,1)S(1)} %collective-permute-done.3.refs_2_), channel_id=1, source_target_pairs={{0,1},{1,0},{2,3},{3,2},{4,5},{5,4},{6,7},{7,6},{8,9},{9,8},{10,11... | collective-permute-start | bytes 1179656 | tf_op jit(solution)/shard_map/ppermute | solution.py:367
  49.1 5.2 %collective-permute-start.8 = (bf16[96,2048]{1,0:T(8,128)(2,1)S(1)}, bf16[96,2048]{1,0:T(8,128)(2,1)S(1)}, u32[]{:S(2)}, u32[]{:S(2)}) collective-permute-start(bf16[96,2048]{1,0:T(8,128)(2,1)S(1)} %collective-permute-done.4.refs_3_), channel_id=1, source_target_pairs={{0,1},{1,0},{2,3},{3,2},{4,5},{5,4},{6,7},{7,6},{8,9},{9,8},{10,11... | collective-permute-start | bytes 1179656 | tf_op jit(solution)/shard_map/ppermute | solution.py:367
  53.8 1.8 %collective-permute-start.9 = (bf16[128,1024]{1,0:T(8,128)(2,1)S(1)}, bf16[128,1024]{1,0:T(8,128)(2,1)S(1)}, u32[]{:S(2)}, u32[]{:S(2)}) collective-permute-start(bf16[128,1024]{1,0:T(8,128)(2,1)S(1)} %get-tuple-element.30), channel_id=1, source_target_pairs={{0,1},{1,0},{2,3},{3,2},{4,5},{5,4},{6,7},{7,6},{8,9},{9,8},{10,11... | collective-permute-start | bytes 786440 | tf_op jit(solution)/shard_map/ppermute | solution.py:367

commit v4 on v3

--- a/solution.py
+++ b/solution.py
@@ -232,13 +232,13 @@
     return wide_s[pl.ds(r * parts + c, peers, stride=slots * parts), :].astype(bf16)
 
 
-def mix_kernel(core, tokens, mine, other, mix_gain, dense_mix, send_map, send, kept, row_gate, wide_s):
+def mix_kernel(tokens, mine, other, mix_gain, dense_mix, send_map, send, kept, row_gate, wide_s):
     half = kept.shape[1]
     attn_out = mine[...].astype(f32) + other[...].astype(f32)
     residual = (tokens[...].astype(f32) + attn_out).astype(bf16)
     rows = residual.astype(f32)
     mixed = (rows * rms(rows) * mix_gain[...]).astype(bf16).astype(f32)
-    first = core[0] == 0
+    first = lax.axis_index("tp") == 0
     kept[...] = jnp.where(first, rows[:, :half], rows[:, half:])
     gate = jnp.zeros((rows.shape[0], LANES), f32)
     for c in range(rows.shape[1] // LANES):
@@ -284,53 +284,39 @@
 
 
 def first_kernel(
-    core, mine, gate_far, up_far, rows_d, gate_part, up_part, gate_back, up_back,
-    wide_s, rows_e, gate, up, sems,
+    mine, gate, up, rows_d, gate_part, up_part, wide_s, rows_e,
 ):
     half = rows_d.shape[1]
-    own = pl.ds(pl.multiple_of(core[0] * half, half), half)
-    back = pl.ds(pl.multiple_of((1 - core[0]) * half, half), half)
-    fetch_gate = pltpu.make_async_copy(gate_far.at[0, own], gate, sems.at[0])
-    fetch_up = pltpu.make_async_copy(up_far.at[0, own], up, sems.at[1])
-    later = [
-        pltpu.make_async_copy(gate_far.at[0, back], gate_back, sems.at[2]),
-        pltpu.make_async_copy(up_far.at[0, back], up_back, sems.at[3]),
-    ]
-    for one in [fetch_gate, fetch_up] + later:
-        one.start()
+    own = pl.ds(pl.multiple_of(lax.axis_index("tp") * half, half), half)
     wide_s[...] = mine[...].astype(f32)
     compact(wide_s, rows_e, rows_d)
-    fetch_gate.wait()
-    gate_part[...] = mm(rows_e[...], gate[...])
-    fetch_up.wait()
-    up_part[...] = mm(rows_e[...], up[...])
-    for one in later:
-        one.wait()
+    gate_part[...] = mm(rows_e[...], gate[0, own])
+    up_part[...] = mm(rows_e[...], up[0, own])
 
 
 def second_kernel(
-    core, other, gate_part, up_part, gate, up, down, rows_d, out_mine, out_other,
+    other, gate_part, up_part, gate, up, down, rows_d, out_mine, out_other,
     wide_s, rows_e, total,
 ):
     half = rows_d.shape[1]
-    at = pl.multiple_of(core[0] * half, half)
-    back = pl.multiple_of((1 - core[0]) * half, half)
+    at = pl.multiple_of(lax.axis_index("tp") * half, half)
+    back = pl.multiple_of((1 - lax.axis_index("tp")) * half, half)
     wide_s[...] = other[...].astype(f32)
     compact(wide_s, rows_e, rows_d)
-    gate_pre = gate_part[...] + mm(rows_e[...], gate[...])
-    up_pre = up_part[...] + mm(rows_e[...], up[...])
+    gate_pre = gate_part[...] + mm(rows_e[...], gate[0, pl.ds(back, half)])
+    up_pre = up_part[...] + mm(rows_e[...], up[0, pl.ds(back, half)])
     hidden = clamped_unit(gate_pre, up_pre).astype(bf16)
     total[...] = mm(hidden, down[0])
     out_mine[...] = total[:, pl.ds(at, half)].astype(bf16)
     out_other[...] = total[:, pl.ds(back, half)].astype(bf16)
 
 
-def dense_kernel(core, mine, other, *refs):
+def dense_kernel(mine, other, *refs):
     packs, out, gate_s, up_s, down_s = refs[:-4], refs[-4], refs[-3], refs[-2], refs[-1]
     half = mine.shape[1]
     units = packs[0].shape[0] // 3
-    at = pl.multiple_of(core[0] * half, half)
-    back = pl.multiple_of((1 - core[0]) * half, half)
+    at = pl.multiple_of(lax.axis_index("tp") * half, half)
+    back = pl.multiple_of((1 - lax.axis_index("tp")) * half, half)
     for i, pack in enumerate(packs):
         to = slice(i * units, (i + 1) * units)
         gate_s[to, :] = pack[0:units, :]
@@ -387,7 +373,6 @@
     seqs, width = tokens.shape
     half, slots, wide = width // 2, CAP * peers, SLOTS * peers
     hidden = expert_gate.shape[2]
-    core = lax.axis_index("tp").astype(jnp.int32).reshape(1)
     pack = jnp.concatenate([dense_gate.T, dense_up.T, dense_down], axis=0)
     pack0 = across(pack, 0)
     part, send_map, home_map = attention(
@@ -402,7 +387,7 @@
     send, kept, row_gate = call(
         mix_kernel,
         (
-            core, tokens, part, far, mix_gain.reshape(1, -1),
+            tokens, part, far, mix_gain.reshape(1, -1),
             dense_mix.reshape(-1, LANES), send_map,
         ),
         [(block, bf16), ((seqs, half), f32), ((seqs, LANES), f32)],
@@ -416,20 +401,16 @@
 
     mine = exchange(send)
     other = swap(mine)
-    rows_mine, gate_part, up_part, gate_back, up_back = call(
+    rows_mine, gate_part, up_part = call(
         first_kernel,
-        (core, mine, expert_gate, expert_up),
-        [((DENSE_ROWS * peers, half), bf16)]
-        + [((slots, hidden), f32)] * 2
-        + [((half, hidden), bf16)] * 2,
-        [(block, f32), ((slots, half), bf16)] + [((half, hidden), bf16)] * 2,
+        (mine, expert_gate, expert_up),
+        [((DENSE_ROWS * peers, half), bf16)] + [((slots, hidden), f32)] * 2,
+        [(block, f32), ((slots, half), bf16)],
         4 * slots * half * hidden,
-        far=2,
-        sems=4,
     )
     rows_other, own, sent = call(
         second_kernel,
-        (core, other, gate_part, up_part, gate_back, up_back, expert_down),
+        (other, gate_part, up_part, expert_gate, expert_up, expert_down),
         [((DENSE_ROWS * peers, half), bf16)] + [((slots, half), bf16)] * 2,
         [(block, f32), ((slots, half), bf16), ((slots, width), f32)],
         8 * slots * half * hidden,
@@ -441,7 +422,7 @@
     units = pack.shape[0] // 3 * len(packs)
     (dense,) = call(
         dense_kernel,
-        (core, rows_mine, rows_other, *packs),
+        (rows_mine, rows_other, *packs),
         [((DENSE_ROWS * peers, half), f32)],
         [((units, width), bf16), ((units, width), bf16), ((units, half), bf16)],
         10 * DENSE_ROWS * peers * half * units,

time: 79 us -> 82.1 us (1.039)
  local copies, waits for them, and re-layouts: 0.03 us -> 3.43 us
  other arithmetic: 0.03 us -> 1.06 us
  waiting for transfers between devices: 25.5 us -> 24.5 us
    unnamed x14 -> x22, local copies, waits for them, and re-layouts: 0.03 us -> 3.43 us
    all_to_all x1, waiting for transfers between devices: 14.8 us -> 13.8 us  [exchange(): return lax.all_to_all(blocks, EP, 0, 0, tiled=True).reshape(block)]
    concatenate x1, other arithmetic: 0.03 us -> 1.06 us  [shards(): pack = jnp.concatenate([dense_gate.T, dense_up.T, dense_down], axis=0)]
  transfers between devices with their start and end apart: 11 -> 11, of which waited for: 4 -> 4; matrix products, arithmetic and copies ran while one was open for 0% -> 1% of each run, Pallas kernels for 7% -> 8%
where the time goes in v4:
time: 82.1 us; the launch traced here: 81.8 us
  waiting for transfers between devices  24.5 us (30%)
  blocking collectives  20.9 us (25%)
  starting transfers between devices  16.6 us (20%)
  Pallas kernels  15.2 us (19%)
  local copies, waits for them, and re-layouts  3.43 us (4%)
  other arithmetic  1.06 us (1%)
    all_to_all x1, blocking collectives, exchange(): return lax.all_to_all(blocks, EP, 0, 0, tiled=True).reshape(block)  20.9 us
    all_to_all x1, waiting for transfers between devices, exchange(): return lax.all_to_all(blocks, EP, 0, 0, tiled=True).reshape(block)  13.8 us
    all_to_all x1, starting transfers between devices, exchange(): return lax.all_to_all(blocks, EP, 0, 0, tiled=True).reshape(block)  11.8 us
    ppermute x3, waiting for transfers between devices, across(): return lax.ppermute(array, ('ep_0', 'ep_1', 'tp'), pairs)  9.45 us
    pallas_call x6, Pallas kernels, call(): pl.pallas_call(kernel, in_specs=[pl.BlockSpec(memory_space=space) for spa...  9.19 us
    pallas_call x1, Pallas kernels, attention(): pl.pallas_call(functools.partial(attention_kernel, peers=peers), in_specs...  6.02 us
    ppermute x3, starting transfers between devices, across(): return lax.ppermute(array, ('ep_0', 'ep_1', 'tp'), pairs)  3.62 us
    unnamed x22, local copies, waits for them, and re-layouts  3.43 us
  transfers between devices with their start and end apart: 11, of which 4 were waited for; matrix products, arithmetic and copies ran while one was open for 1% of the time, Pallas kernels for 8%

profile of v4, /device:TPU:0, one launch (start us, length us, event | category | flops | bytes accessed | tf_op | source)
XLA Modules:
  0.0 81.8 jit_solution(6776883276501840787)
XLA Ops:
  0.0 6.0 %attention.1 = (bf16[16,2048]{1,0:T(8,128)(2,1)S(1)}, bf16[16,384]{1,0:T(8,128)(2,1)S(1)}, bf16[32,384]{1,0:T(8,128)(2,1)S(1)}) custom-call(s32[16]{0:T(128)} %refs_0_.1, f32[4]{0:T(128)} %refs_1_.1, bf16[16,2048]{1,0:T(8,128)(2,1)} %tokens.1, f32[1,2048]{1,0:T(1,128)} %bitcast.25, bf16[2048,256]{1,0:T(8,128)(2,1)} %refs_4_.1, bf16[2048,256]{1,0:T(8,128)(2,1)} %refs_5_.1, ...), custom_call_target="tpu_custom_call" | custom-call | flops 184549376 | bytes 13631488 | tf_op jit(solution)/shard_map/attention/pallas_call | solution.py:195
  6.0 0.1 collective-permute-start
  6.1 1.2 %collective-permute-done.other = bf16[16,2048]{1,0:T(8,128)(2,1)S(1)} collective-permute-done((bf16[16,2048]{1,0:T(8,128)(2,1)S(1)}, bf16[16,2048]{1,0:T(8,128)(2,1)S(1)}, u32[]{:S(2)}, u32[]{:S(2)}) %collective-permute-start) | collective-permute-done | bytes 65568 | tf_op jit(solution)/shard_map/ppermute | solution.py:353
  7.4 0.8 shard_map.235
  8.2 0.9 %copy-done.3 = bf16[3072,128]{1,0:T(8,128)(2,1)} copy-done((bf16[3072,128]{1,0:T(8,128)(2,1)}, bf16[3072,128]{1,0:T(8,128)(2,1)S(1)}, u32[]{:S(2)}) %copy-start.3) | copy-done | bytes 786456
  9.1 0.6 copy-done.5
  9.7 11.8 %all-to-all-start = ((bf16[64,48,128]{2,1,0:T(8,128)(2,1)}), bf16[64,48,128]{2,1,0:T(8,128)(2,1)}, u32[]{:S(2)}, u32[]{:S(2)}) async-start(bf16[64,48,128]{2,1,0:T(8,128)(2,1)} %bitcast.18), calls=%async_computation | async-start | bytes 1572864 | tf_op jit(solution)/shard_map/all_to_all | solution.py:400
  21.5 1.1 %pad_maximum_fusion.refs_0_ = bf16[96,2048]{1,0:T(8,128)(2,1)S(1)} fusion(bf16[32,2048]{1,0:T(8,128)(2,1)} %param.49, bf16[32,2048]{1,0:T(8,128)(2,1)} %bitcast.23, bf16[32,2048]{1,0:T(8,128)(2,1)} %bitcast.24), kind=kLoop, calls=%fused_computation | loop fusion | flops 1179648 | bytes 786432 | tf_op jit(solution)/shard_map/concatenate | solution.py:376
  22.6 1.6 %collective-permute-start.2 = (bf16[96,2048]{1,0:T(8,128)(2,1)S(1)}, bf16[96,2048]{1,0:T(8,128)(2,1)}, u32[]{:S(2)}, u32[]{:S(2)}) collective-permute-start(bf16[96,2048]{1,0:T(8,128)(2,1)S(1)} %pad_maximum_fusion.refs_0_), channel_id=1, source_target_pairs={{0,32},{1,9},{8,40},{9,1},{16,48},{17,25},{24,56},{25,17},{32,0},{... | collective-permute-start | bytes 1179656 | tf_op jit(solution)/shard_map/ppermute | solution.py:364
  24.1 13.8 %all-to-all-done = bf16[64,48,128]{2,1,0:T(8,128)(2,1)} async-done(((bf16[64,48,128]{2,1,0:T(8,128)(2,1)}), bf16[64,48,128]{2,1,0:T(8,128)(2,1)}, u32[]{:S(2)}, u32[]{:S(2)}) %all-to-all-start) | async-done | bytes 786464 | tf_op jit(solution)/shard_map/all_to_all | solution.py:400
  37.9 0.5 collective-permute-start.3
  38.4 1.5 %collective-permute-start.4 = (bf16[96,2048]{1,0:T(8,128)(2,1)}, bf16[96,2048]{1,0:T(8,128)(2,1)S(1)}, u32[]{:S(2)}, u32[]{:S(2)}) collective-permute-start(bf16[96,2048]{1,0:T(8,128)(2,1)} %collective-permute-done.2.refs_1_), channel_id=1, source_target_pairs={{0,8},{1,33},{8,0},{9,41},{16,24},{17,49},{24,16},{25,57},{32,40},... | collective-permute-start | bytes 1179656 | tf_op jit(solution)/shard_map/ppermute | solution.py:364
  40.0 0.5 collective-permute-start.6
  40.5 5.2 %collective-permute-done.3.refs_2_ = bf16[96,2048]{1,0:T(8,128)(2,1)S(1)} collective-permute-done((bf16[96,2048]{1,0:T(8,128)(2,1)S(1)}, bf16[96,2048]{1,0:T(8,128)(2,1)S(1)}, u32[]{:S(2)}, u32[]{:S(2)}) %collective-permute-start.3) | collective-permute-done | bytes 393248 | tf_op jit(solution)/shard_map/ppermute | solution.py:364
  45.7 4.2 %collective-permute-done.4.refs_3_ = bf16[96,2048]{1,0:T(8,128)(2,1)S(1)} collective-permute-done((bf16[96,2048]{1,0:T(8,128)(2,1)}, bf16[96,2048]{1,0:T(8,128)(2,1)S(1)}, u32[]{:S(2)}, u32[]{:S(2)}) %collective-permute-start.4) | collective-permute-done | bytes 393248 | tf_op jit(solution)/shard_map/ppermute | solution.py:364
  49.9 1.9 %copy-done.1 = bf16[1,2048,768]{2,1,0:T(8,128)(2,1)S(1)} copy-done((bf16[1,2048,768]{2,1,0:T(8,128)(2,1)S(1)}, bf16[1,2048,768]{2,1,0:T(8,128)(2,1)}, u32[]{:S(2)}) %copy-start.1) | copy-done | bytes 3145752
  51.8 2.4 %shard_map.236 = (bf16[256,1024]{1,0:T(8,128)(2,1)S(1)}, f32[128,768]{1,0:T(8,128)S(1)}, f32[128,768]{1,0:T(8,128)S(1)}) custom-call(bf16[3072,128]{1,0:T(8,128)(2,1)} %bitcast.11.mine, bf16[1,2048,768]{2,1,0:T(8,128)(2,1)S(1)} %copy-done, bf16[1,2048,768]{2,1,0:T(8,128)(2,1)S(1)} %copy-done.1), custom_call_target="tpu_custom_call" | custom-call | flops 402653184 | bytes 8388608 | tf_op jit(solution)/shard_map/pallas_call | solution.py:262
  54.3 1.7 %shard_map.237 = (bf16[256,1024]{1,0:T(8,128)(2,1)S(1)}, bf16[128,1024]{1,0:T(8,128)(2,1)S(1)}, bf16[128,1024]{1,0:T(8,128)(2,1)S(1)}) custom-call(bf16[3072,128]{1,0:T(8,128)(2,1)S(1)} %collective-permute-done.1.other, f32[128,768]{1,0:T(8,128)S(1)} %get-tuple-element.22.gate_part, f32[128,768]{1,0:T(8,128)S(1)} %get-tuple-element.23.up_part, ...), custom_call_target="tpu_custom_call" | custom-call | flops 805306368 | bytes 12058624 | tf_op jit(solution)/shard_map/pallas_call | solution.py:262
  56.0 0.6 collective-permute-start.9
  56.6 2.2 %shard_map.238.dense = f32[256,1024]{1,0:T(8,128)S(1)} custom-call(bf16[256,1024]{1,0:T(8,128)(2,1)S(1)} %get-tuple-element.21.mine, bf16[256,1024]{1,0:T(8,128)(2,1)S(1)} %get-tuple-element.24.other, bf16[96,2048]{1,0:T(8,128)(2,1)S(1)} %pad_maximum_fusion.refs_0_, bf16[96,2048]{1,0:T(8,128)(2,1)} %collective-permute-done.2.refs_1_, ...), custom_call_target="tpu_custom_call" | custom-call | flops 671088640 | bytes 5242880 | tf_op jit(solution)/shard_map/pallas_call | solution.py:262
  58.8 0.0 copy-start.8
  58.8 0.6 shard_map.239
  59.4 20.9 %all_to_all.10 = bf16[64,48,128]{2,1,0:T(8,128)(2,1)S(1)} all-to-all(bf16[64,48,128]{2,1,0:T(8,128)(2,1)S(1)} %bitcast.17), channel_id=1, replica_groups=mesh['ep_0'=4,'ep_1'=4,'ep_2'=4,'tp'=2] {'ep_0','ep_1','ep_2'}, dimensions={0} | all-to-all | bytes 1572864 | tf_op jit(solution)/shard_map/all_to_all | solution.py:400
  80.3 1.5 %shard_map.240 = bf16[16,1024]{1,0:T(8,128)(2,1)} custom-call(bf16[32,384]{1,0:T(8,128)(2,1)S(1)} %copy-done.8, bf16[3072,128]{1,0:T(8,128)(2,1)S(1)} %bitcast.16, f32[16,1024]{1,0:T(8,128)S(1)} %copy-done.6, f32[16,128]{1,0:T(8,128)S(1)} %get-tuple-element.28.row_gate), custom_call_target="tpu_custom_call" | custom-call | flops 25165824 | bytes 917504 | tf_op jit(solution)/shard_map/pallas_call | solution.py:262
  (29 shorter events, 0.1 us)
Async XLA Ops:
  0.0 7.4 %copy-start.4 = (bf16[16,2048]{1,0:T(8,128)(2,1)S(1)}, bf16[16,2048]{1,0:T(8,128)(2,1)}, u32[]{:S(2)}) copy-start(bf16[16,2048]{1,0:T(8,128)(2,1)} %tokens.1) | copy-start | bytes 196612
  0.0 7.4 %copy-start.9 = (f32[2048]{0:T(1024)S(1)}, f32[2048]{0:T(1024)}, u32[]{:S(2)}) copy-start(f32[2048]{0:T(1024)} %param.40) | copy-start | bytes 24580
  0.0 7.4 %copy-start.10 = (bf16[2048]{0:T(1024)(128)(2,1)S(1)}, bf16[2048]{0:T(1024)(128)(2,1)}, u32[]{:S(2)}) copy-start(bf16[2048]{0:T(1024)(128)(2,1)} %param.46) | copy-start | bytes 12292
  0.0 49.9 %copy-start = (bf16[1,2048,768]{2,1,0:T(8,128)(2,1)S(1)}, bf16[1,2048,768]{2,1,0:T(8,128)(2,1)}, u32[]{:S(2)}) copy-start(bf16[1,2048,768]{2,1,0:T(8,128)(2,1)} %gate.3) | copy-start | bytes 9437188
  6.0 2.2 %copy-start.7 = (bf16[32,384]{1,0:T(8,128)(2,1)}, bf16[32,384]{1,0:T(8,128)(2,1)S(1)}, u32[]{:S(2)}) copy-start(bf16[32,384]{1,0:T(8,128)(2,1)S(1)} %get-tuple-element.17.home_map) | copy-start | bytes 73732
  6.0 1.3 %collective-permute-start = (bf16[16,2048]{1,0:T(8,128)(2,1)S(1)}, bf16[16,2048]{1,0:T(8,128)(2,1)S(1)}, u32[]{:S(2)}, u32[]{:S(2)}) collective-permute-start(bf16[16,2048]{1,0:T(8,128)(2,1)S(1)} %get-tuple-element.18.mine), channel_id=1, source_target_pairs={{0,1},{1,0},{2,3},{3,2},{4,5},{5,4},{6,7},{7,6},{8,9},{9,8},{10,11... | collective-permute-start | bytes 196616 | tf_op jit(solution)/shard_map/ppermute | solution.py:353
  8.2 0.9 %copy-start.3 = (bf16[3072,128]{1,0:T(8,128)(2,1)}, bf16[3072,128]{1,0:T(8,128)(2,1)S(1)}, u32[]{:S(2)}) copy-start(bf16[3072,128]{1,0:T(8,128)(2,1)S(1)} %get-tuple-element.20) | copy-start | bytes 2359300
  9.1 0.6 copy-start.5
  9.7 28.2 %all-to-all-start = ((bf16[64,48,128]{2,1,0:T(8,128)(2,1)}), bf16[64,48,128]{2,1,0:T(8,128)(2,1)}, u32[]{:S(2)}, u32[]{:S(2)}) async-start(bf16[64,48,128]{2,1,0:T(8,128)(2,1)} %bitcast.18), calls=%async_computation | async-start | bytes 1572864 | tf_op jit(solution)/shard_map/all_to_all | solution.py:400
  22.6 15.9 %collective-permute-start.2 = (bf16[96,2048]{1,0:T(8,128)(2,1)S(1)}, bf16[96,2048]{1,0:T(8,128)(2,1)}, u32[]{:S(2)}, u32[]{:S(2)}) collective-permute-start(bf16[96,2048]{1,0:T(8,128)(2,1)S(1)} %pad_maximum_fusion.refs_0_), channel_id=1, source_target_pairs={{0,32},{1,9},{8,40},{9,1},{16,48},{17,25},{24,56},{25,17},{32,0},{... | collective-permute-start | bytes 1179656 | tf_op jit(solution)/shard_map/ppermute | solution.py:364
  37.9 16.3 %collective-permute-start.1 = (bf16[3072,128]{1,0:T(8,128)(2,1)}, bf16[3072,128]{1,0:T(8,128)(2,1)S(1)}, u32[]{:S(2)}, u32[]{:S(2)}) collective-permute-start(bf16[3072,128]{1,0:T(8,128)(2,1)} %bitcast.11.mine), channel_id=1, source_target_pairs={{0,1},{1,0},{2,3},{3,2},{4,5},{5,4},{6,7},{7,6},{8,9},{9,8},{10,11... | collective-permute-start | bytes 2359304 | tf_op jit(solution)/shard_map/ppermute | solution.py:353
  37.9 7.8 %collective-permute-start.3 = (bf16[96,2048]{1,0:T(8,128)(2,1)S(1)}, bf16[96,2048]{1,0:T(8,128)(2,1)S(1)}, u32[]{:S(2)}, u32[]{:S(2)}) collective-permute-start(bf16[96,2048]{1,0:T(8,128)(2,1)S(1)} %pad_maximum_fusion.refs_0_), channel_id=1, source_target_pairs={{0,8},{1,33},{8,0},{9,41},{16,24},{17,49},{24,16},{25,57},{32,40},... | collective-permute-start | bytes 1179656 | tf_op jit(solution)/shard_map/ppermute | solution.py:364
  38.4 11.5 %collective-permute-start.4 = (bf16[96,2048]{1,0:T(8,128)(2,1)}, bf16[96,2048]{1,0:T(8,128)(2,1)S(1)}, u32[]{:S(2)}, u32[]{:S(2)}) collective-permute-start(bf16[96,2048]{1,0:T(8,128)(2,1)} %collective-permute-done.2.refs_1_), channel_id=1, source_target_pairs={{0,8},{1,33},{8,0},{9,41},{16,24},{17,49},{24,16},{25,57},{32,40},... | collective-permute-start | bytes 1179656 | tf_op jit(solution)/shard_map/ppermute | solution.py:364
  39.9 16.7 %collective-permute-start.5 = (bf16[96,2048]{1,0:T(8,128)(2,1)S(1)}, bf16[96,2048]{1,0:T(8,128)(2,1)S(1)}, u32[]{:S(2)}, u32[]{:S(2)}) collective-permute-start(bf16[96,2048]{1,0:T(8,128)(2,1)S(1)} %pad_maximum_fusion.refs_0_), channel_id=1, source_target_pairs={{0,1},{1,0},{2,3},{3,2},{4,5},{5,4},{6,7},{7,6},{8,9},{9,8},{10,11... | collective-permute-start | bytes 1179656 | tf_op jit(solution)/shard_map/ppermute | solution.py:353
  40.0 16.7 %collective-permute-start.6 = (bf16[96,2048]{1,0:T(8,128)(2,1)}, bf16[96,2048]{1,0:T(8,128)(2,1)S(1)}, u32[]{:S(2)}, u32[]{:S(2)}) collective-permute-start(bf16[96,2048]{1,0:T(8,128)(2,1)} %collective-permute-done.2.refs_1_), channel_id=1, source_target_pairs={{0,1},{1,0},{2,3},{3,2},{4,5},{5,4},{6,7},{7,6},{8,9},{9,8},{10,11... | collective-permute-start | bytes 1179656 | tf_op jit(solution)/shard_map/ppermute | solution.py:353
  45.7 10.9 %collective-permute-start.7 = (bf16[96,2048]{1,0:T(8,128)(2,1)S(1)}, bf16[96,2048]{1,0:T(8,128)(2,1)S(1)}, u32[]{:S(2)}, u32[]{:S(2)}) collective-permute-start(bf16[96,2048]{1,0:T(8,128)(2,1)S(1)} %collective-permute-done.3.refs_2_), channel_id=1, source_target_pairs={{0,1},{1,0},{2,3},{3,2},{4,5},{5,4},{6,7},{7,6},{8,9},{9,8},{10,11... | collective-permute-start | bytes 1179656 | tf_op jit(solution)/shard_map/ppermute | solution.py:353
  49.9 6.7 %collective-permute-start.8 = (bf16[96,2048]{1,0:T(8,128)(2,1)S(1)}, bf16[96,2048]{1,0:T(8,128)(2,1)S(1)}, u32[]{:S(2)}, u32[]{:S(2)}) collective-permute-start(bf16[96,2048]{1,0:T(8,128)(2,1)S(1)} %collective-permute-done.4.refs_3_), channel_id=1, source_target_pairs={{0,1},{1,0},{2,3},{3,2},{4,5},{5,4},{6,7},{7,6},{8,9},{9,8},{10,11... | collective-permute-start | bytes 1179656 | tf_op jit(solution)/shard_map/ppermute | solution.py:353
  49.9 1.9 %copy-start.1 = (bf16[1,2048,768]{2,1,0:T(8,128)(2,1)S(1)}, bf16[1,2048,768]{2,1,0:T(8,128)(2,1)}, u32[]{:S(2)}) copy-start(bf16[1,2048,768]{2,1,0:T(8,128)(2,1)} %up.3) | copy-start | bytes 9437188
  51.8 2.5 %copy-start.2 = (bf16[1,768,2048]{2,1,0:T(8,128)(2,1)S(1)}, bf16[1,768,2048]{2,1,0:T(8,128)(2,1)}, u32[]{:S(2)}) copy-start(bf16[1,768,2048]{2,1,0:T(8,128)(2,1)} %down.1) | copy-start | bytes 9437188
  56.0 2.8 %collective-permute-start.9 = (bf16[128,1024]{1,0:T(8,128)(2,1)S(1)}, bf16[128,1024]{1,0:T(8,128)(2,1)S(1)}, u32[]{:S(2)}, u32[]{:S(2)}) collective-permute-start(bf16[128,1024]{1,0:T(8,128)(2,1)S(1)} %get-tuple-element.26), channel_id=1, source_target_pairs={{0,1},{1,0},{2,3},{3,2},{4,5},{5,4},{6,7},{7,6},{8,9},{9,8},{10,11... | collective-permute-start | bytes 786440 | tf_op jit(solution)/shard_map/ppermute | solution.py:353
  58.8 21.5 %copy-start.6 = (f32[16,1024]{1,0:T(8,128)S(1)}, f32[16,1024]{1,0:T(8,128)}, u32[]{:S(2)}) copy-start(f32[16,1024]{1,0:T(8,128)} %copy-done.5) | copy-start | bytes 196612
  58.8 21.5 %copy-start.8 = (bf16[32,384]{1,0:T(8,128)(2,1)S(1)}, bf16[32,384]{1,0:T(8,128)(2,1)}, u32[]{:S(2)}) copy-start(bf16[32,384]{1,0:T(8,128)(2,1)} %copy-done.7) | copy-start | bytes 73732

commit v5 on v4

--- a/solution.py
+++ b/solution.py
@@ -82,13 +82,14 @@
 
 
 def attention_kernel(*refs, peers):
-    sources, refs = refs[:17], refs[17:]
+    w_query1, w_query2, w_key1, w_key2, w_value, w_output = refs[:6]
+    sources, refs = refs[6:17], refs[17:]
     part, send_map, home_map = refs[:3]
     query_s, key_s, value_s, heads_s, *local = refs[3:-1]
     sems = refs[-1]
     (
-        lengths, lam, tokens, attn_gain, w_query1, w_query2, w_key1, w_key2, w_value, query_gain, key_gain,
-        routes_t, weight_t, sub_gain, w_output, cache_key, cache_value,
+        lengths, lam, tokens, attn_gain, query_gain, key_gain, routes_t, weight_t, sub_gain,
+        cache_key, cache_value,
     ) = local
     seqs = tokens.shape[0]
     heads = w_query1.shape[1] // HEAD
@@ -102,12 +103,12 @@
         of = pl.ds(b * SEQ_STEP, SEQ_STEP)
         for j in (0, 1):
             at = len(copies) + len(chunks)
-            source, to = sources[15 + j].at[of], local[15 + j].at[of]
+            source, to = sources[9 + j].at[of], local[9 + j].at[of]
             chunks.append(pltpu.make_async_copy(source, to, sems.at[at]))
-    for one in copies[:-1] + chunks + copies[-1:]:
+    for one in copies + chunks:
         one.start()
 
-    for one in copies[:-1]:
+    for one in copies:
         one.wait()
     rows = tokens[...].astype(f32)
     normed = (rows * rms(rows) * attn_gain[...]).astype(bf16)
@@ -171,7 +172,6 @@
     for h in range(heads):
         one = heads_s[h * seqs : (h + 1) * seqs, :]
         subs.append((one * rms(one) * sub_gain[...] * (1.0 - lambda_start)).astype(bf16))
-    copies[-1].wait()
     part[...] = mm(jnp.concatenate(subs, axis=1), w_output[...]).astype(bf16)
 
 
@@ -184,17 +184,19 @@
     heads = w_query1.shape[1] // HEAD
     cached = cache_key.shape[2]
     local = [
-        lengths, head_lambda, tokens, attn_gain.reshape(1, -1), w_query1, w_query2, w_key1.T, w_key2.T, w_value,
-        query_gain.reshape(1, -1), key_gain.reshape(1, -1), routes.T, route_weight.T,
-        sub_gain.reshape(1, -1), w_output, cache_key, cache_value,
+        lengths, head_lambda, tokens, attn_gain.reshape(1, -1), query_gain.reshape(1, -1),
+        key_gain.reshape(1, -1), routes.T, route_weight.T, sub_gain.reshape(1, -1), cache_key,
+        cache_value,
     ]
+    near = [w_query1, w_query2, w_key1.T, w_key2.T, w_value, w_output]
     flops = 2 * seqs * width * (2 * heads * HEAD + 2 * HEAD + VHEAD + heads * VHEAD)
     flops += 6 * seqs * 8 * cached * VHEAD
     wide = peers * SLOTS
     count = len(local) - 2 + 2 * (seqs // SEQ_STEP)
     return pl.pallas_call(
         functools.partial(attention_kernel, peers=peers),
-        in_specs=[pl.BlockSpec(memory_space=pltpu.HBM)] * len(local),
+        in_specs=[pl.BlockSpec(memory_space=pltpu.VMEM)] * len(near)
+        + [pl.BlockSpec(memory_space=pltpu.HBM)] * len(local),
         out_specs=[pl.BlockSpec(memory_space=pltpu.VMEM)] * 3,
         out_shape=[
             pltpu.VMEM((seqs, width), bf16),
@@ -215,7 +217,7 @@
             flops=flops, bytes_accessed=13 << 20, transcendentals=seqs * 8 * cached
         ),
         name="attention",
-    )(*[pltpu.with_memory_space_constraint(one, pltpu.HBM) for one in local])
+    )(*near, *[pltpu.with_memory_space_constraint(one, pltpu.HBM) for one in local])
 
 
 def spread(wide_s, rows, first):
@@ -311,6 +313,18 @@
     out_other[...] = total[:, pl.ds(back, half)].astype(bf16)
 
 
+def pack_kernel(gate, up, down, out, sems):
+    units = gate.shape[0]
+    copies = [
+        pltpu.make_async_copy(one, out.at[pl.ds(i * units, units)], sems.at[i])
+        for i, one in enumerate((gate, up, down))
+    ]
+    for one in copies:
+        one.start()
+    for one in copies:
+        one.wait()
+
+
 def dense_kernel(mine, other, *refs):
     packs, out, gate_s, up_s, down_s = refs[:-4], refs[-4], refs[-3], refs[-2], refs[-1]
     half = mine.shape[1]
@@ -373,7 +387,16 @@
     seqs, width = tokens.shape
     half, slots, wide = width // 2, CAP * peers, SLOTS * peers
     hidden = expert_gate.shape[2]
-    pack = jnp.concatenate([dense_gate.T, dense_up.T, dense_down], axis=0)
+    units = dense_down.shape[0]
+    (pack,) = call(
+        pack_kernel,
+        (dense_gate.T, dense_up.T, dense_down),
+        [((3 * units, width), bf16)],
+        [],
+        1 << 34,
+        far=3,
+        sems=3,
+    )
     pack0 = across(pack, 0)
     part, send_map, home_map = attention(
         tokens, attn_gain, w_query1, w_query2, w_key1, w_key2, w_value, query_gain,

time: 82.1 us -> 88 us (1.072)
  local copies, waits for them, and re-layouts: 3.43 us -> 9.52 us
  other arithmetic: 1.06 us -> 0 us
    unnamed x22 -> x32, local copies, waits for them, and re-layouts: 3.43 us -> 9.52 us
    pallas_call x6 -> x7, Pallas kernels: 9.19 us -> 11.2 us  [call(): pl.pallas_call(kernel, in_specs=[pl.BlockSpec(memory_space=space) for spa...]
    pallas_call x1, Pallas kernels: 6.02 us -> 4.8 us  [attention(): pl.pallas_call(functools.partial(attention_kernel, peers=peers), in_specs...]
    concatenate x1 -> x0, other arithmetic: 1.06 us -> none  [shards(): pack = jnp.concatenate([dense_gate.T, dense_up.T, dense_down], axis=0)]
  transfers between devices with their start and end apart: 11 -> 11, of which waited for: 4 -> 4; matrix products, arithmetic and copies ran while one was open for 1% -> 0% of each run, Pallas kernels for 8% -> 9%
where the time goes in v5:
time: 88 us; the launch traced here: 87.4 us
  waiting for transfers between devices  24.3 us (28%)
  blocking collectives  20.9 us (24%)
  starting transfers between devices  16.6 us (19%)
  Pallas kernels  16 us (18%)
  local copies, waits for them, and re-layouts  9.52 us (11%)
    all_to_all x1, blocking collectives, exchange(): return lax.all_to_all(blocks, EP, 0, 0, tiled=True).reshape(block)  20.9 us
    all_to_all x1, waiting for transfers between devices, exchange(): return lax.all_to_all(blocks, EP, 0, 0, tiled=True).reshape(block)  13.6 us
    all_to_all x1, starting transfers between devices, exchange(): return lax.all_to_all(blocks, EP, 0, 0, tiled=True).reshape(block)  11.8 us
    pallas_call x7, Pallas kernels, call(): pl.pallas_call(kernel, in_specs=[pl.BlockSpec(memory_space=space) for spa...  11.2 us
    unnamed x32, local copies, waits for them, and re-layouts  9.52 us
    ppermute x3, waiting for transfers between devices, across(): return lax.ppermute(array, ('ep_0', 'ep_1', 'tp'), pairs)  9.45 us
    pallas_call x1, Pallas kernels, attention(): pl.pallas_call(functools.partial(attention_kernel, peers=peers), in_specs...  4.8 us
    ppermute x3, starting transfers between devices, across(): return lax.ppermute(array, ('ep_0', 'ep_1', 'tp'), pairs)  3.62 us
  transfers between devices with their start and end apart: 11, of which 4 were waited for; matrix products, arithmetic and copies ran while one was open for 0% of the time, Pallas kernels for 9%

profile of v5, /device:TPU:0, one launch (start us, length us, event | category | flops | bytes accessed | tf_op | source)
XLA Modules:
  0.0 87.4 jit_solution(1185448768257396338)
XLA Ops:
  0.0 1.6 %copy-done.3 = bf16[512,2048]{1,0:T(8,128)(2,1)S(1)} copy-done((bf16[512,2048]{1,0:T(8,128)(2,1)S(1)}, bf16[512,2048]{1,0:T(8,128)(2,1)}, u32[]{:S(2)}) %copy-start.3) | copy-done | bytes 2097176
  1.6 1.2 %copy-done.4 = bf16[2048,256]{1,0:T(8,128)(2,1)S(1)} copy-done((bf16[2048,256]{1,0:T(8,128)(2,1)S(1)}, bf16[2048,256]{1,0:T(8,128)(2,1)}, u32[]{:S(2)}) %copy-start.4) | copy-done | bytes 1048600
  2.8 1.2 %copy-done.5 = bf16[2048,256]{1,0:T(8,128)(2,1)S(1)} copy-done((bf16[2048,256]{1,0:T(8,128)(2,1)S(1)}, bf16[2048,256]{1,0:T(8,128)(2,1)}, u32[]{:S(2)}) %copy-start.5) | copy-done | bytes 1048600
  4.0 1.0 %copy-done.6 = bf16[2048,128]{1,0:T(8,128)(2,1)S(1)} copy-done((bf16[2048,128]{1,0:T(8,128)(2,1)S(1)}, bf16[2048,128]{1,0:T(8,128)(2,1)}, u32[]{:S(2)}) %copy-start.6) | copy-done | bytes 524312
  5.1 0.9 %copy-done.8 = bf16[2048,64]{0,1:T(8,128)(2,1)S(1)} copy-done((bf16[2048,64]{0,1:T(8,128)(2,1)S(1)}, bf16[2048,64]{0,1:T(8,128)(2,1)}, u32[]{:S(2)}) %copy-start.8) | copy-done | bytes 262168
  6.0 0.9 %copy-done.9 = bf16[2048,64]{0,1:T(8,128)(2,1)S(1)} copy-done((bf16[2048,64]{0,1:T(8,128)(2,1)S(1)}, bf16[2048,64]{0,1:T(8,128)(2,1)}, u32[]{:S(2)}) %copy-start.9) | copy-done | bytes 262168
  7.0 4.8 %attention.1 = (bf16[16,2048]{1,0:T(8,128)(2,1)S(1)}, bf16[16,384]{1,0:T(8,128)(2,1)S(1)}, bf16[32,384]{1,0:T(8,128)(2,1)S(1)}) custom-call(bf16[2048,256]{1,0:T(8,128)(2,1)S(1)} %copy-done.4, bf16[2048,256]{1,0:T(8,128)(2,1)S(1)} %copy-done.5, bf16[64,2048]{1,0:T(8,128)(2,1)S(1)} %bitcast.18, bf16[64,2048]{1,0:T(8,128)(2,1)S(1)} %bitcast.19, ...), custom_call_target="tpu_custom_call" | custom-call | flops 184549376 | bytes 13631488 | tf_op jit(solution)/shard_map/attention/pallas_call | solution.py:196
  11.9 1.2 %collective-permute-done.other = bf16[16,2048]{1,0:T(8,128)(2,1)S(1)} collective-permute-done((bf16[16,2048]{1,0:T(8,128)(2,1)S(1)}, bf16[16,2048]{1,0:T(8,128)(2,1)S(1)}, u32[]{:S(2)}, u32[]{:S(2)}) %collective-permute-start) | collective-permute-done | bytes 65568 | tf_op jit(solution)/shard_map/ppermute | solution.py:367
  13.2 1.7 %shard_map.235 = (bf16[3072,128]{1,0:T(8,128)(2,1)}, f32[16,1024]{1,0:T(8,128)S(1)}, f32[16,128]{1,0:T(8,128)S(1)}) custom-call(bf16[16,2048]{1,0:T(8,128)(2,1)S(1)} %copy-done.7, bf16[16,2048]{1,0:T(8,128)(2,1)S(1)} %get-tuple-element.18.mine, bf16[16,2048]{1,0:T(8,128)(2,1)S(1)} %collective-permute-done.other, f32[1,2048]{1,0:T(1,128)S(1)} %bitcast.20, ...), custom_call_target="tpu_custom_call" | custom-call | flops 12582912 | bytes 1081344 | tf_op jit(solution)/shard_map/pallas_call | solution.py:264
  14.9 0.6 copy-done.10
  15.5 11.8 %all-to-all-start = ((bf16[64,48,128]{2,1,0:T(8,128)(2,1)}), bf16[64,48,128]{2,1,0:T(8,128)(2,1)}, u32[]{:S(2)}, u32[]{:S(2)}) async-start(bf16[64,48,128]{2,1,0:T(8,128)(2,1)} %bitcast.10), calls=%async_computation | async-start | bytes 1572864 | tf_op jit(solution)/shard_map/all_to_all | solution.py:423
  27.2 1.2 %shard_map.238.refs_0_ = bf16[96,2048]{1,0:T(8,128)(2,1)S(1)} custom-call(bf16[32,2048]{1,0:T(8,128)(2,1)} %bitcast.28, bf16[32,2048]{1,0:T(8,128)(2,1)} %bitcast.29, bf16[32,2048]{1,0:T(8,128)(2,1)} %down.3), custom_call_target="tpu_custom_call" | custom-call | flops 17179869184 | bytes 786432 | tf_op jit(solution)/shard_map/pallas_call | solution.py:264
  28.5 1.6 %collective-permute-start.2 = (bf16[96,2048]{1,0:T(8,128)(2,1)S(1)}, bf16[96,2048]{1,0:T(8,128)(2,1)}, u32[]{:S(2)}, u32[]{:S(2)}) collective-permute-start(bf16[96,2048]{1,0:T(8,128)(2,1)S(1)} %shard_map.238.refs_0_), channel_id=1, source_target_pairs={{0,32},{1,9},{8,40},{9,1},{16,48},{17,25},{24,56},{25,17},{32,0},{... | collective-permute-start | bytes 1179656 | tf_op jit(solution)/shard_map/ppermute | solution.py:378
  30.1 13.6 %all-to-all-done = bf16[64,48,128]{2,1,0:T(8,128)(2,1)} async-done(((bf16[64,48,128]{2,1,0:T(8,128)(2,1)}), bf16[64,48,128]{2,1,0:T(8,128)(2,1)}, u32[]{:S(2)}, u32[]{:S(2)}) %all-to-all-start) | async-done | bytes 786464 | tf_op jit(solution)/shard_map/all_to_all | solution.py:423
  44.2 1.5 %collective-permute-start.4 = (bf16[96,2048]{1,0:T(8,128)(2,1)}, bf16[96,2048]{1,0:T(8,128)(2,1)S(1)}, u32[]{:S(2)}, u32[]{:S(2)}) collective-permute-start(bf16[96,2048]{1,0:T(8,128)(2,1)} %collective-permute-done.2.refs_1_), channel_id=1, source_target_pairs={{0,8},{1,33},{8,0},{9,41},{16,24},{17,49},{24,16},{25,57},{32,40},... | collective-permute-start | bytes 1179656 | tf_op jit(solution)/shard_map/ppermute | solution.py:378
  46.2 5.2 %collective-permute-done.3.refs_2_ = bf16[96,2048]{1,0:T(8,128)(2,1)S(1)} collective-permute-done((bf16[96,2048]{1,0:T(8,128)(2,1)S(1)}, bf16[96,2048]{1,0:T(8,128)(2,1)S(1)}, u32[]{:S(2)}, u32[]{:S(2)}) %collective-permute-start.3) | collective-permute-done | bytes 393248 | tf_op jit(solution)/shard_map/ppermute | solution.py:378
  51.4 4.2 %collective-permute-done.4.refs_3_ = bf16[96,2048]{1,0:T(8,128)(2,1)S(1)} collective-permute-done((bf16[96,2048]{1,0:T(8,128)(2,1)}, bf16[96,2048]{1,0:T(8,128)(2,1)S(1)}, u32[]{:S(2)}, u32[]{:S(2)}) %collective-permute-start.4) | collective-permute-done | bytes 393248 | tf_op jit(solution)/shard_map/ppermute | solution.py:378
  55.7 1.9 %copy-done.1 = bf16[1,2048,768]{2,1,0:T(8,128)(2,1)S(1)} copy-done((bf16[1,2048,768]{2,1,0:T(8,128)(2,1)S(1)}, bf16[1,2048,768]{2,1,0:T(8,128)(2,1)}, u32[]{:S(2)}) %copy-start.1) | copy-done | bytes 3145752
  57.5 2.4 %shard_map.236 = (bf16[256,1024]{1,0:T(8,128)(2,1)S(1)}, f32[128,768]{1,0:T(8,128)S(1)}, f32[128,768]{1,0:T(8,128)S(1)}) custom-call(bf16[3072,128]{1,0:T(8,128)(2,1)} %bitcast.11.mine, bf16[1,2048,768]{2,1,0:T(8,128)(2,1)S(1)} %copy-done, bf16[1,2048,768]{2,1,0:T(8,128)(2,1)S(1)} %copy-done.1), custom_call_target="tpu_custom_call" | custom-call | flops 402653184 | bytes 8388608 | tf_op jit(solution)/shard_map/pallas_call | solution.py:264
  60.0 1.7 %shard_map.237 = (bf16[256,1024]{1,0:T(8,128)(2,1)S(1)}, bf16[128,1024]{1,0:T(8,128)(2,1)S(1)}, bf16[128,1024]{1,0:T(8,128)(2,1)S(1)}) custom-call(bf16[3072,128]{1,0:T(8,128)(2,1)S(1)} %collective-permute-done.1.other, f32[128,768]{1,0:T(8,128)S(1)} %get-tuple-element.22.gate_part, f32[128,768]{1,0:T(8,128)S(1)} %get-tuple-element.23.up_part, ...), custom_call_target="tpu_custom_call" | custom-call | flops 805306368 | bytes 12058624 | tf_op jit(solution)/shard_map/pallas_call | solution.py:264
  61.7 0.6 collective-permute-start.9
  62.3 2.2 %shard_map.239.dense = f32[256,1024]{1,0:T(8,128)S(1)} custom-call(bf16[256,1024]{1,0:T(8,128)(2,1)S(1)} %get-tuple-element.21.mine, bf16[256,1024]{1,0:T(8,128)(2,1)S(1)} %get-tuple-element.24.other, bf16[96,2048]{1,0:T(8,128)(2,1)S(1)} %shard_map.238.refs_0_, bf16[96,2048]{1,0:T(8,128)(2,1)} %collective-permute-done.2.refs_1_, ...), custom_call_target="tpu_custom_call" | custom-call | flops 671088640 | bytes 5242880 | tf_op jit(solution)/shard_map/pallas_call | solution.py:264
  65.1 20.9 %all_to_all.10 = bf16[64,48,128]{2,1,0:T(8,128)(2,1)S(1)} all-to-all(bf16[64,48,128]{2,1,0:T(8,128)(2,1)S(1)} %bitcast.17), channel_id=1, replica_groups=mesh['ep_0'=4,'ep_1'=4,'ep_2'=4,'tp'=2] {'ep_0','ep_1','ep_2'}, dimensions={0} | all-to-all | bytes 1572864 | tf_op jit(solution)/shard_map/all_to_all | solution.py:423
  86.0 1.5 %shard_map.241 = bf16[16,1024]{1,0:T(8,128)(2,1)} custom-call(bf16[32,384]{1,0:T(8,128)(2,1)S(1)} %copy-done.13, bf16[3072,128]{1,0:T(8,128)(2,1)S(1)} %bitcast.16, f32[16,1024]{1,0:T(8,128)S(1)} %copy-done.11, f32[16,128]{1,0:T(8,128)S(1)} %get-tuple-element.28.row_gate), custom_call_target="tpu_custom_call" | custom-call | flops 25165824 | bytes 917504 | tf_op jit(solution)/shard_map/pallas_call | solution.py:264
  (39 shorter events, 1.7 us)
Async XLA Ops:
  0.0 1.6 %copy-start.3 = (bf16[512,2048]{1,0:T(8,128)(2,1)S(1)}, bf16[512,2048]{1,0:T(8,128)(2,1)}, u32[]{:S(2)}) copy-start(bf16[512,2048]{1,0:T(8,128)(2,1)} %refs_5_.1) | copy-start | bytes 6291460
  1.6 1.2 %copy-start.4 = (bf16[2048,256]{1,0:T(8,128)(2,1)S(1)}, bf16[2048,256]{1,0:T(8,128)(2,1)}, u32[]{:S(2)}) copy-start(bf16[2048,256]{1,0:T(8,128)(2,1)} %refs_0_.1) | copy-start | bytes 3145732
  2.8 1.2 %copy-start.5 = (bf16[2048,256]{1,0:T(8,128)(2,1)S(1)}, bf16[2048,256]{1,0:T(8,128)(2,1)}, u32[]{:S(2)}) copy-start(bf16[2048,256]{1,0:T(8,128)(2,1)} %refs_1_.1) | copy-start | bytes 3145732
  4.0 1.0 %copy-start.6 = (bf16[2048,128]{1,0:T(8,128)(2,1)S(1)}, bf16[2048,128]{1,0:T(8,128)(2,1)}, u32[]{:S(2)}) copy-start(bf16[2048,128]{1,0:T(8,128)(2,1)} %refs_4_.1) | copy-start | bytes 1572868
  7.0 6.2 %copy-start.7 = (bf16[16,2048]{1,0:T(8,128)(2,1)S(1)}, bf16[16,2048]{1,0:T(8,128)(2,1)}, u32[]{:S(2)}) copy-start(bf16[16,2048]{1,0:T(8,128)(2,1)} %tokens.1) | copy-start | bytes 196612
  7.0 6.2 %copy-start.14 = (f32[2048]{0:T(1024)S(1)}, f32[2048]{0:T(1024)}, u32[]{:S(2)}) copy-start(f32[2048]{0:T(1024)} %param.40) | copy-start | bytes 24580
  7.0 6.2 %copy-start.15 = (bf16[2048]{0:T(1024)(128)(2,1)S(1)}, bf16[2048]{0:T(1024)(128)(2,1)}, u32[]{:S(2)}) copy-start(bf16[2048]{0:T(1024)(128)(2,1)} %param.46) | copy-start | bytes 12292
  11.8 3.0 %copy-start.12 = (bf16[32,384]{1,0:T(8,128)(2,1)}, bf16[32,384]{1,0:T(8,128)(2,1)S(1)}, u32[]{:S(2)}) copy-start(bf16[32,384]{1,0:T(8,128)(2,1)S(1)} %get-tuple-element.17.home_map) | copy-start | bytes 73732
  11.8 1.3 %collective-permute-start = (bf16[16,2048]{1,0:T(8,128)(2,1)S(1)}, bf16[16,2048]{1,0:T(8,128)(2,1)S(1)}, u32[]{:S(2)}, u32[]{:S(2)}) collective-permute-start(bf16[16,2048]{1,0:T(8,128)(2,1)S(1)} %get-tuple-element.18.mine), channel_id=1, source_target_pairs={{0,1},{1,0},{2,3},{3,2},{4,5},{5,4},{6,7},{7,6},{8,9},{9,8},{10,11... | collective-permute-start | bytes 196616 | tf_op jit(solution)/shard_map/ppermute | solution.py:367
  15.5 28.2 %all-to-all-start = ((bf16[64,48,128]{2,1,0:T(8,128)(2,1)}), bf16[64,48,128]{2,1,0:T(8,128)(2,1)}, u32[]{:S(2)}, u32[]{:S(2)}) async-start(bf16[64,48,128]{2,1,0:T(8,128)(2,1)} %bitcast.10), calls=%async_computation | async-start | bytes 1572864 | tf_op jit(solution)/shard_map/all_to_all | solution.py:423
  27.2 28.4 %copy-start = (bf16[1,2048,768]{2,1,0:T(8,128)(2,1)S(1)}, bf16[1,2048,768]{2,1,0:T(8,128)(2,1)}, u32[]{:S(2)}) copy-start(bf16[1,2048,768]{2,1,0:T(8,128)(2,1)} %gate.3) | copy-start | bytes 9437188
  28.5 15.7 %collective-permute-start.2 = (bf16[96,2048]{1,0:T(8,128)(2,1)S(1)}, bf16[96,2048]{1,0:T(8,128)(2,1)}, u32[]{:S(2)}, u32[]{:S(2)}) collective-permute-start(bf16[96,2048]{1,0:T(8,128)(2,1)S(1)} %shard_map.238.refs_0_), channel_id=1, source_target_pairs={{0,32},{1,9},{8,40},{9,1},{16,48},{17,25},{24,56},{25,17},{32,0},{... | collective-permute-start | bytes 1179656 | tf_op jit(solution)/shard_map/ppermute | solution.py:378
  43.7 16.3 %collective-permute-start.1 = (bf16[3072,128]{1,0:T(8,128)(2,1)}, bf16[3072,128]{1,0:T(8,128)(2,1)S(1)}, u32[]{:S(2)}, u32[]{:S(2)}) collective-permute-start(bf16[3072,128]{1,0:T(8,128)(2,1)} %bitcast.11.mine), channel_id=1, source_target_pairs={{0,1},{1,0},{2,3},{3,2},{4,5},{5,4},{6,7},{7,6},{8,9},{9,8},{10,11... | collective-permute-start | bytes 2359304 | tf_op jit(solution)/shard_map/ppermute | solution.py:367
  43.7 7.8 %collective-permute-start.3 = (bf16[96,2048]{1,0:T(8,128)(2,1)S(1)}, bf16[96,2048]{1,0:T(8,128)(2,1)S(1)}, u32[]{:S(2)}, u32[]{:S(2)}) collective-permute-start(bf16[96,2048]{1,0:T(8,128)(2,1)S(1)} %shard_map.238.refs_0_), channel_id=1, source_target_pairs={{0,8},{1,33},{8,0},{9,41},{16,24},{17,49},{24,16},{25,57},{32,40},... | collective-permute-start | bytes 1179656 | tf_op jit(solution)/shard_map/ppermute | solution.py:378
  44.2 11.5 %collective-permute-start.4 = (bf16[96,2048]{1,0:T(8,128)(2,1)}, bf16[96,2048]{1,0:T(8,128)(2,1)S(1)}, u32[]{:S(2)}, u32[]{:S(2)}) collective-permute-start(bf16[96,2048]{1,0:T(8,128)(2,1)} %collective-permute-done.2.refs_1_), channel_id=1, source_target_pairs={{0,8},{1,33},{8,0},{9,41},{16,24},{17,49},{24,16},{25,57},{32,40},... | collective-permute-start | bytes 1179656 | tf_op jit(solution)/shard_map/ppermute | solution.py:378
  45.7 16.6 %collective-permute-start.5 = (bf16[96,2048]{1,0:T(8,128)(2,1)S(1)}, bf16[96,2048]{1,0:T(8,128)(2,1)S(1)}, u32[]{:S(2)}, u32[]{:S(2)}) collective-permute-start(bf16[96,2048]{1,0:T(8,128)(2,1)S(1)} %shard_map.238.refs_0_), channel_id=1, source_target_pairs={{0,1},{1,0},{2,3},{3,2},{4,5},{5,4},{6,7},{7,6},{8,9},{9,8},{10,11... | collective-permute-start | bytes 1179656 | tf_op jit(solution)/shard_map/ppermute | solution.py:367
  45.7 16.6 %collective-permute-start.6 = (bf16[96,2048]{1,0:T(8,128)(2,1)}, bf16[96,2048]{1,0:T(8,128)(2,1)S(1)}, u32[]{:S(2)}, u32[]{:S(2)}) collective-permute-start(bf16[96,2048]{1,0:T(8,128)(2,1)} %collective-permute-done.2.refs_1_), channel_id=1, source_target_pairs={{0,1},{1,0},{2,3},{3,2},{4,5},{5,4},{6,7},{7,6},{8,9},{9,8},{10,11... | collective-permute-start | bytes 1179656 | tf_op jit(solution)/shard_map/ppermute | solution.py:367
  51.4 10.9 %collective-permute-start.7 = (bf16[96,2048]{1,0:T(8,128)(2,1)S(1)}, bf16[96,2048]{1,0:T(8,128)(2,1)S(1)}, u32[]{:S(2)}, u32[]{:S(2)}) collective-permute-start(bf16[96,2048]{1,0:T(8,128)(2,1)S(1)} %collective-permute-done.3.refs_2_), channel_id=1, source_target_pairs={{0,1},{1,0},{2,3},{3,2},{4,5},{5,4},{6,7},{7,6},{8,9},{9,8},{10,11... | collective-permute-start | bytes 1179656 | tf_op jit(solution)/shard_map/ppermute | solution.py:367
  55.6 6.7 %collective-permute-start.8 = (bf16[96,2048]{1,0:T(8,128)(2,1)S(1)}, bf16[96,2048]{1,0:T(8,128)(2,1)S(1)}, u32[]{:S(2)}, u32[]{:S(2)}) collective-permute-start(bf16[96,2048]{1,0:T(8,128)(2,1)S(1)} %collective-permute-done.4.refs_3_), channel_id=1, source_target_pairs={{0,1},{1,0},{2,3},{3,2},{4,5},{5,4},{6,7},{7,6},{8,9},{9,8},{10,11... | collective-permute-start | bytes 1179656 | tf_op jit(solution)/shard_map/ppermute | solution.py:367
  55.7 1.9 %copy-start.1 = (bf16[1,2048,768]{2,1,0:T(8,128)(2,1)S(1)}, bf16[1,2048,768]{2,1,0:T(8,128)(2,1)}, u32[]{:S(2)}) copy-start(bf16[1,2048,768]{2,1,0:T(8,128)(2,1)} %up.3) | copy-start | bytes 9437188
  57.5 2.4 %copy-start.2 = (bf16[1,768,2048]{2,1,0:T(8,128)(2,1)S(1)}, bf16[1,768,2048]{2,1,0:T(8,128)(2,1)}, u32[]{:S(2)}) copy-start(bf16[1,768,2048]{2,1,0:T(8,128)(2,1)} %down.2) | copy-start | bytes 9437188
  61.7 2.8 %collective-permute-start.9 = (bf16[128,1024]{1,0:T(8,128)(2,1)S(1)}, bf16[128,1024]{1,0:T(8,128)(2,1)S(1)}, u32[]{:S(2)}, u32[]{:S(2)}) collective-permute-start(bf16[128,1024]{1,0:T(8,128)(2,1)S(1)} %get-tuple-element.26), channel_id=1, source_target_pairs={{0,1},{1,0},{2,3},{3,2},{4,5},{5,4},{6,7},{7,6},{8,9},{9,8},{10,11... | collective-permute-start | bytes 786440 | tf_op jit(solution)/shard_map/ppermute | solution.py:367
  64.5 21.5 %copy-start.11 = (f32[16,1024]{1,0:T(8,128)S(1)}, f32[16,1024]{1,0:T(8,128)}, u32[]{:S(2)}) copy-start(f32[16,1024]{1,0:T(8,128)} %copy-done.10) | copy-start | bytes 196612
  64.5 21.5 %copy-start.13 = (bf16[32,384]{1,0:T(8,128)(2,1)S(1)}, bf16[32,384]{1,0:T(8,128)(2,1)}, u32[]{:S(2)}) copy-start(bf16[32,384]{1,0:T(8,128)(2,1)} %copy-done.12) | copy-start | bytes 73732
  (3 other events, 2.5 us)
